TPU v7x, 128 devices: a whole 4x4x4 slice. The times are simulated.
128 devices in a mesh: tp: 16 (over z, x), dp: 8 (over y, core).
Axes of the slice: x: 4, y: 4, z: 4, core: 2. Of those that a mesh axis runs over, the one named last changes fastest.
Arguments:
- tokens: bfloat16 [256, 4096], P('tp', 'dp'), may hold values from -6 to 6
- query_weight: bfloat16 [2, 4096, 2048], P(None, 'dp', 'tp'), may hold values from -0.09375 to 0.09375
- key_weight: bfloat16 [2, 4096, 2048], P(None, 'dp', 'tp'), may hold values from -0.09375 to 0.09375
- value_weight: bfloat16 [2, 4096, 2048], P(None, 'dp', 'tp'), may hold values from -0.09375 to 0.09375
- outgate_weight: bfloat16 [2, 4096, 2048], P(None, 'dp', 'tp'), may hold values from -0.09375 to 0.09375
- igate_weight: bfloat16 [2, 4096, 16], replicated, may hold values from -0.09375 to 0.09375
- fgate_weight: bfloat16 [2, 4096, 16], replicated, may hold values from -0.09375 to 0.09375
- norm_gain: float32 [2, 4096], P(None, 'dp'), may hold values from 0.1 to 1.9
- head_gain: float32 [2, 2048], P(None, 'tp'), may hold values from 0.1 to 1.9
- proj_weight: bfloat16 [2, 2048, 4096], P(None, 'tp', 'dp'), may hold values from -0.125 to 0.125
- cell_state: float32 [2, 256, 16, 128, 128], P(None, 'dp', 'tp'), may hold values from -1.8 to 1.8
- normer_state: float32 [2, 256, 16, 128], P(None, 'dp', 'tp'), may hold values from -1.8 to 1.8
- stab_state: float32 [2, 256, 16], P(None, 'dp', 'tp'), may hold values from -4 to 4
Outputs:
- final_rows: bfloat16 [256, 4096], P('tp', 'dp')
- cell_out: float32 [2, 256, 16, 128, 128], P(None, 'dp', 'tp')
- normer_out: float32 [2, 256, 16, 128], P(None, 'dp', 'tp')
- stab_out: float32 [2, 256, 16], P(None, 'dp', 'tp')
All inputs are finite; a program needn't handle non-finite values.
Results may differ from a plain program's by a relative error of at most 0.012.
The roundings to bfloat16 on the way count: a program that leaves them out, or rounds other values in their place, can miss the bound.
Values may be sent and summed in bfloat16 or wider, within the bound.
A program may use at most 64 MiB of HBM per device.

v0:
```python
import jax
import jax.numpy as jnp
from jax import lax
from jax.sharding import PartitionSpec as P

D = 4096


EPSILON = 1e-06


def joined_along(parts, dim):
    shape = list(parts.shape[1:])
    shape[dim] *= parts.shape[0]
    return jnp.moveaxis(parts, 0, dim).reshape(shape)


def from_everyone(array, axis):
    copies = jnp.broadcast_to(array, (lax.axis_size(axis), *array.shape))
    return lax.all_to_all(copies, axis, split_axis=0, concat_axis=0, tiled=True)


def gather_directly(array, axis, dim):
    return joined_along(from_everyone(array, axis), dim)


def in_blocks(array, dim, length):
    before, after = (array.shape[:dim], array.shape[dim + 1 :])
    return jnp.moveaxis(array.reshape(*before, length, -1, *after), dim, 0)


def sum_at_owner(array, axis, dim):
    parts = in_blocks(array, dim, lax.axis_size(axis))
    arrived = lax.all_to_all(parts, axis, split_axis=0, concat_axis=0, tiled=True)
    return arrived.sum(axis=0)


def in_one_piece(arrays, axis, dim, along):
    columns = [a.reshape(*a.shape[:along], -1) for a in arrays]
    both = jnp.concatenate(columns, axis=along)
    out, at, gathered = (sum_at_owner(both, axis, dim), 0, [])
    for a, column in zip(arrays, columns):
        slab = out[..., at : at + column.shape[along]]
        gathered.append(slab.reshape(*slab.shape[:along], *a.shape[along:]))
        at += column.shape[along]
    return tuple(gathered)


def gather_rows(block_input):
    return gather_directly(block_input, "tp", 0)


def spread_heads(out_part):
    return sum_at_owner(out_part, "tp", 0)


def per_device(
    tokens,
    query_weight,
    key_weight,
    value_weight,
    outgate_weight,
    igate_weight,
    fgate_weight,
    norm_gain,
    head_gain,
    proj_weight,
    cell_state,
    normer_state,
    stab_state,
):
    dp_rank = lax.axis_index("dp")
    tp_rank = lax.axis_index("tp")
    local_seqs = cell_state.shape[1]
    local_heads = cell_state.shape[2]
    head_dim = cell_state.shape[3]
    row_width = query_weight.shape[1]
    num_blocks = query_weight.shape[0]
    gathered = gather_rows(tokens)
    final_rows = tokens
    cell_list = []
    normer_list = []
    stab_list = []
    for layer_num in range(num_blocks):
        as_float = gathered.astype(jnp.float32)
        part_squares = jnp.sum(as_float * as_float, axis=1)
        scaled = (as_float * norm_gain[layer_num]).astype(jnp.bfloat16)

        def product(weight):
            return jnp.dot(scaled, weight, preferred_element_type=jnp.float32)

        gate_start = (dp_rank * row_width, tp_rank * local_heads)
        igate_rows = lax.dynamic_slice(
            igate_weight[layer_num], gate_start, (row_width, local_heads)
        )
        fgate_rows = lax.dynamic_slice(
            fgate_weight[layer_num], gate_start, (row_width, local_heads)
        )
        query_part = product(query_weight[layer_num])
        key_part = product(key_weight[layer_num])
        value_part = product(value_weight[layer_num])
        outgate_part = product(outgate_weight[layer_num])
        igate_part = product(igate_rows)
        forget_part = product(fgate_rows)
        query_sum, key_sum, value_sum, outgate_sum, igate_sum, forget_sum, own_sq = in_one_piece(
            (query_part, key_part, value_part, outgate_part, igate_part, forget_part, part_squares),
            "dp",
            0,
            1,
        )
        inv_rms = lax.rsqrt(own_sq / D + EPSILON)[:, None]
        query_rows = (query_sum * inv_rms).reshape(local_seqs, local_heads, head_dim)
        key_rows = (key_sum * inv_rms * head_dim ** (-0.5)).reshape(
            local_seqs, local_heads, head_dim
        )
        value_rows = (value_sum * inv_rms).reshape(local_seqs, local_heads, head_dim)
        outgate = outgate_sum * inv_rms
        igate = igate_sum * inv_rms
        forget = jax.nn.log_sigmoid(forget_sum * inv_rms)
        prev_stab = stab_state[layer_num]
        new_stab = jnp.maximum(forget + prev_stab, igate)
        keep_rate = jnp.exp(forget + prev_stab - new_stab)
        write_rate = jnp.exp(igate - new_stab)
        new_cell = (
            keep_rate[..., None, None] * cell_state[layer_num]
            + write_rate[..., None, None] * value_rows[..., :, None] * key_rows[..., None, :]
        )
        new_normer = (
            keep_rate[..., None] * normer_state[layer_num] + write_rate[..., None] * key_rows
        )
        numerator = jnp.einsum(
            "bhvd,bhd->bhv", new_cell, query_rows, precision=lax.Precision.HIGHEST
        )
        denominator = jnp.maximum(jnp.abs(jnp.sum(new_normer * query_rows, axis=-1)), 1.0)
        readout = numerator / denominator[..., None]
        normed = readout * lax.rsqrt(jnp.mean(readout * readout, axis=-1, keepdims=True) + EPSILON)
        normed = normed * head_gain[layer_num].reshape(local_heads, head_dim)
        gated_out = (
            jax.nn.sigmoid(outgate) * normed.reshape(local_seqs, local_heads * head_dim)
        ).astype(jnp.bfloat16)
        all_gated = gather_directly(gated_out, "dp", 0)
        out_part = jnp.dot(all_gated, proj_weight[layer_num], preferred_element_type=jnp.float32)
        if layer_num + 1 < num_blocks:
            gathered = gather_rows(spread_heads(out_part).astype(jnp.bfloat16))
        else:
            final_rows = spread_heads(out_part).astype(jnp.bfloat16)
        cell_list.append(new_cell)
        normer_list.append(new_normer)
        stab_list.append(new_stab)
    return (final_rows, jnp.stack(cell_list), jnp.stack(normer_list), jnp.stack(stab_list))


def solution(mesh):
    return jax.shard_map(
        per_device,
        mesh=mesh,
        in_specs=(
            P("tp", "dp"),
            P(None, "dp", "tp"),
            P(None, "dp", "tp"),
            P(None, "dp", "tp"),
            P(None, "dp", "tp"),
            P(),
            P(),
            P(None, "dp"),
            P(None, "tp"),
            P(None, "tp", "dp"),
            P(None, "dp", "tp", None, None),
            P(None, "dp", "tp", None),
            P(None, "dp", "tp"),
        ),
        out_specs=(
            P("tp", "dp"),
            P(None, "dp", "tp", None, None),
            P(None, "dp", "tp", None),
            P(None, "dp", "tp"),
        ),
        check_vma=False,
    )
```

profile of v0, /device:TPU:1, one launch (start us, length us, event | category | flops | bytes accessed | tf_op | source)
XLA Modules:
  0.0 127.8 jit_solution(3152498219810558530)
XLA Ops:
  0.7 1.5 %broadcast_in_dim.8 = bf16[16,16,512]{2,1,0:T(8,128)(2,1)} broadcast(bf16[16,512]{1,0:T(8,128)(2,1)} %param.13), dimensions={1,2} | broadcast | bytes 278528 | tf_op jit(solution)/shard_map/broadcast_in_dim | solution.py:19
  2.2 8.4 %all-to-all-start = ((bf16[16,16,512]{2,1,0:T(8,128)(2,1)}), bf16[16,16,512]{2,1,0:T(8,128)(2,1)S(1)}, u32[]{:S(2)}, u32[]{:S(2)}) async-start(bf16[16,16,512]{2,1,0:T(8,128)(2,1)} %broadcast_in_dim.8), calls=%async_computation | async-start | bytes 524288 | tf_op jit(solution)/shard_map/all_to_all | solution.py:20
  10.6 1.0 fusion.97
  11.6 1.0 fusion.96
  12.6 0.8 fusion.98
  13.4 4.8 %all-to-all-done = bf16[16,16,512]{2,1,0:T(8,128)(2,1)S(1)} async-done(((bf16[16,16,512]{2,1,0:T(8,128)(2,1)}), bf16[16,16,512]{2,1,0:T(8,128)(2,1)S(1)}, u32[]{:S(2)}, u32[]{:S(2)}) %all-to-all-start) | async-done | bytes 262176 | tf_op jit(solution)/shard_map/all_to_all | solution.py:20
  19.9 1.0 concatenate.13
  20.9 6.6 %all-to-all-start.1 = ((f32[8,32,515]{2,1,0:T(8,128)}), f32[8,32,515]{2,1,0:T(8,128)S(1)}, u32[]{:S(2)}, u32[]{:S(2)}) async-start(f32[8,32,515]{2,1,0:T(8,128)} %concatenate.13), calls=%async_computation.1 | async-start | bytes 1310720 | tf_op jit(solution)/shard_map/all_to_all | solution.py:34
  27.6 10.6 %all-to-all-done.1 = f32[8,32,515]{2,1,0:T(8,128)S(1)} async-done(((f32[8,32,515]{2,1,0:T(8,128)}), f32[8,32,515]{2,1,0:T(8,128)S(1)}, u32[]{:S(2)}, u32[]{:S(2)}) %all-to-all-start.1) | async-done | bytes 527392 | tf_op jit(solution)/shard_map/all_to_all | solution.py:34
  38.8 5.1 %fusion.4 = f32[32,1,128]{2,1,0:T(1,128)S(1)} fusion(f32[32,128,1]{1,2,0:T(1,128)S(1)} %bitcast.172, f32[2,32,1,128,128]{4,3,2,1,0:T(8,128)} %param.23, f32[32,128]{1,0:T(8,128)S(1)} %get-tuple-element.47, f32[32,128]{1,0:T(8,128)S(1)} %get-tuple-element.46, f32[32]{0:T(128)S(1)} %get-tuple-element.21), kind=kOutput, calls=%fused_computation.6 | convolution fusion | flops 7864320 | bytes 2162816 | tf_op jit(solution)/shard_map/bhvd,bhd->bhv/dot_general | solution.py:131
  44.2 8.2 %all_to_all.40 = bf16[8,32,128]{2,1,0:T(8,128)(2,1)S(1)} all-to-all(bf16[8,32,128]{2,1,0:T(8,128)(2,1)S(1)} %broadcast_in_dim.9), channel_id=1, replica_groups=mesh['tp'=16,'dp'=8] {'dp'}, dimensions={0} | all-to-all | bytes 131072 | tf_op jit(solution)/shard_map/all_to_all | solution.py:20
  52.6 13.2 %all_to_all.41 = f32[16,16,512]{2,1,0:T(8,128)S(1)} all-to-all(f32[16,16,512]{2,1,0:T(8,128)S(1)} %fusion.30), channel_id=1, replica_groups=mesh['tp'=16,'dp'=8] {'tp'}, dimensions={0} | all-to-all | bytes 1048576 | tf_op jit(solution)/shard_map/all_to_all | solution.py:34
  65.9 10.6 %all_to_all.42 = bf16[16,16,512]{2,1,0:T(8,128)(2,1)S(1)} all-to-all(bf16[16,16,512]{2,1,0:T(8,128)(2,1)S(1)} %broadcast_in_dim.10), channel_id=1, replica_groups=mesh['tp'=16,'dp'=8] {'tp'}, dimensions={0} | all-to-all | bytes 524288 | tf_op jit(solution)/shard_map/all_to_all | solution.py:20
  78.2 1.0 concatenate.15
  79.2 6.3 %all-to-all-start.5 = ((f32[8,32,515]{2,1,0:T(8,128)}), f32[8,32,515]{2,1,0:T(8,128)S(1)}, u32[]{:S(2)}, u32[]{:S(2)}) async-start(f32[8,32,515]{2,1,0:T(8,128)} %concatenate.15), calls=%async_computation.5 | async-start | bytes 1310720 | tf_op jit(solution)/shard_map/all_to_all | solution.py:34
  85.6 10.7 %all-to-all-done.5 = f32[8,32,515]{2,1,0:T(8,128)S(1)} async-done(((f32[8,32,515]{2,1,0:T(8,128)}), f32[8,32,515]{2,1,0:T(8,128)S(1)}, u32[]{:S(2)}, u32[]{:S(2)}) %all-to-all-start.5) | async-done | bytes 527392 | tf_op jit(solution)/shard_map/all_to_all | solution.py:34
  96.8 5.1 %fusion.1 = f32[32,1,128]{2,1,0:T(1,128)S(1)} fusion(f32[32,128,1]{1,2,0:T(1,128)S(1)} %bitcast.173, f32[2,32,1,128,128]{4,3,2,1,0:T(8,128)} %param.23, f32[32,128]{1,0:T(8,128)S(1)} %get-tuple-element.45, f32[32,128]{1,0:T(8,128)S(1)} %get-tuple-element.44, f32[32]{0:T(128)S(1)} %get-tuple-element.24), kind=kOutput, calls=%fused_computation.3 | convolution fusion | flops 7864320 | bytes 2162816 | tf_op jit(solution)/shard_map/bhvd,bhd->bhv/dot_general | solution.py:131
  102.9 4.2 %all-to-all-start.6 = ((bf16[8,32,128]{2,1,0:T(8,128)(2,1)}), bf16[8,32,128]{2,1,0:T(8,128)(2,1)S(1)}, u32[]{:S(2)}, u32[]{:S(2)}) async-start(bf16[8,32,128]{2,1,0:T(8,128)(2,1)} %broadcast_in_dim.11), calls=%async_computation.6 | async-start | bytes 131072 | tf_op jit(solution)/shard_map/all_to_all | solution.py:20
  108.3 3.7 %all-to-all-done.6 = bf16[8,32,128]{2,1,0:T(8,128)(2,1)S(1)} async-done(((bf16[8,32,128]{2,1,0:T(8,128)(2,1)}), bf16[8,32,128]{2,1,0:T(8,128)(2,1)S(1)}, u32[]{:S(2)}, u32[]{:S(2)}) %all-to-all-start.6) | async-done | bytes 65568 | tf_op jit(solution)/shard_map/all_to_all | solution.py:20
  112.0 1.0 fusion.20
  113.0 3.6 %all-to-all-start.7 = ((f32[16,16,512]{2,1,0:T(8,128)}), f32[16,16,512]{2,1,0:T(8,128)S(1)}, u32[]{:S(2)}, u32[]{:S(2)}) async-start(f32[16,16,512]{2,1,0:T(8,128)} %fusion.20), calls=%async_computation.7 | async-start | bytes 1048576 | tf_op jit(solution)/shard_map/all_to_all | solution.py:34
  116.5 3.0 %multiply_add_fusion.1 = (f32[1,32,1,128,128]{4,3,2,1,0:T(8,128)S(1)}, f32[1,32,1,128,128]{4,3,2,1,0:T(8,128)S(1)}) fusion(f32[2,32,1,128,128]{4,3,2,1,0:T(8,128)} %param.23, f32[32,128]{1,0:T(8,128)S(1)} %get-tuple-element.47, f32[32,128]{1,0:T(8,128)S(1)} %get-tuple-element.46, f32[32]{0:T(128)S(1)} %get-tuple-element.21, ...), kind=kLoop, calls=%fused_computation.8 | loop fusion | flops 3145728 | bytes 8454400 | tf_op jit(solution)/shard_map/add | solution.py:125
  119.5 2.3 %pad_maximum_fusion = f32[2,32,1,128,128]{4,3,2,1,0:T(8,128)} fusion(f32[1,32,1,128,128]{4,3,2,1,0:T(8,128)S(1)} %get-tuple-element.33, f32[1,32,1,128,128]{4,3,2,1,0:T(8,128)S(1)} %get-tuple-element.32), kind=kLoop, calls=%fused_computation | loop fusion | flops 1048576 | bytes 8388608 | tf_op jit(solution)/shard_map/stack | solution.py:150
  121.8 5.3 %all-to-all-done.7 = f32[16,16,512]{2,1,0:T(8,128)S(1)} async-done(((f32[16,16,512]{2,1,0:T(8,128)}), f32[16,16,512]{2,1,0:T(8,128)S(1)}, u32[]{:S(2)}, u32[]{:S(2)}) %all-to-all-start.7) | async-done | bytes 524320 | tf_op jit(solution)/shard_map/all_to_all | solution.py:34
  (60 shorter events, 7.9 us)
Async XLA Ops:
  0.6 17.8 %copy-start = (bf16[2,512,128]{2,1,0:T(8,128)(2,1)S(1)}, bf16[2,512,128]{2,1,0:T(8,128)(2,1)}, u32[]{:S(2)}) copy-start(bf16[2,512,128]{2,1,0:T(8,128)(2,1)} %param.17) | copy-start | bytes 786436
  0.6 18.0 %copy-start.1 = (bf16[2,512,128]{2,1,0:T(8,128)(2,1)S(1)}, bf16[2,512,128]{2,1,0:T(8,128)(2,1)}, u32[]{:S(2)}) copy-start(bf16[2,512,128]{2,1,0:T(8,128)(2,1)} %param.16) | copy-start | bytes 786436
  0.7 18.2 %copy-start.2 = (bf16[2,512,128]{2,1,0:T(8,128)(2,1)S(1)}, bf16[2,512,128]{2,1,0:T(8,128)(2,1)}, u32[]{:S(2)}) copy-start(bf16[2,512,128]{2,1,0:T(8,128)(2,1)} %param.15) | copy-start | bytes 786436
  0.7 18.5 %copy-start.3 = (bf16[2,512,128]{2,1,0:T(8,128)(2,1)S(1)}, bf16[2,512,128]{2,1,0:T(8,128)(2,1)}, u32[]{:S(2)}) copy-start(bf16[2,512,128]{2,1,0:T(8,128)(2,1)} %param.14) | copy-start | bytes 786436
  2.2 16.0 %all-to-all-start = ((bf16[16,16,512]{2,1,0:T(8,128)(2,1)}), bf16[16,16,512]{2,1,0:T(8,128)(2,1)S(1)}, u32[]{:S(2)}, u32[]{:S(2)}) async-start(bf16[16,16,512]{2,1,0:T(8,128)(2,1)} %broadcast_in_dim.8), calls=%async_computation | async-start | bytes 524288 | tf_op jit(solution)/shard_map/all_to_all | solution.py:20
  19.1 8.4 %copy-start.6 = (f32[2,32,1]{1,2,0:T(1,128)S(1)}, f32[2,32,1]{1,2,0:T(1,128)}, u32[]{:S(2)}) copy-start(f32[2,32,1]{1,2,0:T(1,128)} %param.25) | copy-start | bytes 772
  19.1 8.5 %copy-start.7 = (f32[2,128]{1,0:T(2,128)S(1)}, f32[2,128]{1,0:T(2,128)}, u32[]{:S(2)}) copy-start(f32[2,128]{1,0:T(2,128)} %param.21) | copy-start | bytes 3076
  19.6 18.9 %copy-start.5 = (f32[2,32,1,128]{3,2,1,0:T(1,128)S(1)}, f32[2,32,1,128]{3,2,1,0:T(1,128)}, u32[]{:S(2)}) copy-start(f32[2,32,1,128]{3,2,1,0:T(1,128)} %param.24) | copy-start | bytes 98308
  20.9 17.3 %all-to-all-start.1 = ((f32[8,32,515]{2,1,0:T(8,128)}), f32[8,32,515]{2,1,0:T(8,128)S(1)}, u32[]{:S(2)}, u32[]{:S(2)}) async-start(f32[8,32,515]{2,1,0:T(8,128)} %concatenate.13), calls=%async_computation.1 | async-start | bytes 1310720 | tf_op jit(solution)/shard_map/all_to_all | solution.py:34
  27.5 24.9 %copy-start.4 = (bf16[2,128,512]{2,1,0:T(8,128)(2,1)S(1)}, bf16[2,128,512]{2,1,0:T(8,128)(2,1)}, u32[]{:S(2)}) copy-start(bf16[2,128,512]{2,1,0:T(8,128)(2,1)} %param.22) | copy-start | bytes 786436
  79.2 17.1 %all-to-all-start.5 = ((f32[8,32,515]{2,1,0:T(8,128)}), f32[8,32,515]{2,1,0:T(8,128)S(1)}, u32[]{:S(2)}, u32[]{:S(2)}) async-start(f32[8,32,515]{2,1,0:T(8,128)} %concatenate.15), calls=%async_computation.5 | async-start | bytes 1310720 | tf_op jit(solution)/shard_map/all_to_all | solution.py:34
  102.9 9.1 %all-to-all-start.6 = ((bf16[8,32,128]{2,1,0:T(8,128)(2,1)}), bf16[8,32,128]{2,1,0:T(8,128)(2,1)S(1)}, u32[]{:S(2)}, u32[]{:S(2)}) async-start(bf16[8,32,128]{2,1,0:T(8,128)(2,1)} %broadcast_in_dim.11), calls=%async_computation.6 | async-start | bytes 131072 | tf_op jit(solution)/shard_map/all_to_all | solution.py:20
  113.0 14.2 %all-to-all-start.7 = ((f32[16,16,512]{2,1,0:T(8,128)}), f32[16,16,512]{2,1,0:T(8,128)S(1)}, u32[]{:S(2)}, u32[]{:S(2)}) async-start(f32[16,16,512]{2,1,0:T(8,128)} %fusion.20), calls=%async_computation.7 | async-start | bytes 1048576 | tf_op jit(solution)/shard_map/all_to_all | solution.py:34
where the time goes:
time: 129 us; the launch traced here: 128 us
  waiting for transfers between devices  35.1 us (27%)
  blocking collectives  32 us (25%)
  starting transfers between devices  29.1 us (23%)
  matrix products  14.2 us (11%)
  other arithmetic  9.01 us (7%)
  local copies, waits for them, and re-layouts  7.31 us (6%)
    all_to_all x3, waiting for transfers between devices, sum_at_owner(): lax.all_to_all(parts, axis, split_axis=0, concat_axis=0, tiled=True)  26.7 us
    all_to_all x2, blocking collectives, from_everyone(): return lax.all_to_all(copies, axis, split_axis=0, concat_axis=0, tiled=True)  18.8 us
    all_to_all x3, starting transfers between devices, sum_at_owner(): lax.all_to_all(parts, axis, split_axis=0, concat_axis=0, tiled=True)  16.5 us
    all_to_all x1, blocking collectives, sum_at_owner(): lax.all_to_all(parts, axis, split_axis=0, concat_axis=0, tiled=True)  13.2 us
    all_to_all x2, starting transfers between devices, from_everyone(): return lax.all_to_all(copies, axis, split_axis=0, concat_axis=0, tiled=True)  12.6 us
    dot_general x2, matrix products, per_device(): jnp.einsum('bhvd,bhd->bhv', new_cell, query_rows, precision=lax.Precision...  10.2 us
    all_to_all x2, waiting for transfers between devices, from_everyone(): return lax.all_to_all(copies, axis, split_axis=0, concat_axis=0, tiled=True)  8.47 us
    add x1, other arithmetic, per_device(): keep_rate[..., None, None] * cell_state[layer_num]  2.98 us
  transfers between devices with their start and end apart: 5, of which 5 were waited for; matrix products, arithmetic and copies ran while one was open for 7% of the time, Pallas kernels for 0%

commit v1 on v0

v1 whole, which is shorter than its diff:
```python
import functools

import jax
import jax.numpy as jnp
from jax import lax
from jax.experimental import pallas as pl
from jax.experimental.pallas import tpu as pltpu
from jax.sharding import PartitionSpec as P

D = 4096
EPSILON = 1e-06
NB = 2
TP = 16
DP = 8
ROWS = 256
DH = 128
SIDE = 4
COLS = 512
TROWS = ROWS // TP
DROWS = ROWS // DP
QKVO = 4 * DH
SEMS = 13
PIECES = 8

F32 = jnp.float32
BF16 = jnp.bfloat16


def ring_distance(step):
    return min(step, SIDE - step)


TP_STEPS = sorted(
    ((dz, dx) for dz in range(SIDE) for dx in range(SIDE) if (dz, dx) != (0, 0)),
    key=lambda s: -(ring_distance(s[0]) + ring_distance(s[1])),
)
DP_STEPS = sorted(
    ((dy, dc) for dy in range(SIDE) for dc in range(2) if (dy, dc) != (0, 0)),
    key=lambda s: -(2 * ring_distance(s[0]) + s[1]),
)


def dot_nt(a, b):
    return lax.dot_general(a, b, (((1,), (1,)), ((), ())), preferred_element_type=F32)


def mega(
    tok,
    qw,
    kw,
    vw,
    ow,
    igt,
    fgt,
    ngain,
    hgain,
    pw,
    cell,
    normer,
    stab,
    final_out,
    cell_out,
    normer_out,
    stab_out,
    g,
    w,
    gates,
    grow,
    pwv,
    ngv,
    hgv,
    n0v,
    m0v,
    cv,
    chl,
    scaled,
    dsend,
    drecv,
    ysend,
    yrecv,
    qs,
    wvt,
    gat,
    osend0,
    osend1,
    orecv0,
    orecv1,
    fin,
    n1v,
    m1v,
    lsem,
    wsem,
    ssem,
    rsem,
):
    me_t = lax.axis_index("tp")
    me_d = lax.axis_index("dp")
    z, x = me_t // SIDE, me_t % SIDE
    y, core = me_d // 2, me_d % 2
    tp_peers = [((z + dz) % SIDE) * SIDE + (x + dx) % SIDE for dz, dx in TP_STEPS]
    dp_peers = [((y + dy) % SIDE) * 2 + (core + dc) % 2 for dy, dc in DP_STEPS]
    y_peers = [(y + dy) % SIDE for dy in (2, 1, 3)]
    partner = y * 2 + 1 - core
    own_t = pl.ds(pl.multiple_of(me_t * TROWS, TROWS), TROWS)
    own_d = pl.ds(pl.multiple_of(me_d * DROWS, DROWS), DROWS)
    own_cols = pl.ds(pl.multiple_of(me_d * COLS, COLS), COLS)

    loads = [pltpu.make_async_copy(tok, g.at[0, own_t], lsem.at[0])]
    loads.append(pltpu.make_async_copy(ngain, ngv, lsem.at[1]))
    loads.append(pltpu.make_async_copy(igt.at[:, :, own_cols], gates.at[0], lsem.at[2]))
    loads.append(pltpu.make_async_copy(fgt.at[:, :, own_cols], gates.at[1], lsem.at[3]))
    for i, src in enumerate((qw, kw, vw, ow)):
        loads.append(
            pltpu.make_async_copy(src, w.at[:, :, pl.ds(i * DH, DH)], lsem.at[4 + i])
        )
    loads.append(pltpu.make_async_copy(pw, pwv, lsem.at[8]))
    loads.append(pltpu.make_async_copy(hgain, hgv, lsem.at[9]))
    loads.append(pltpu.make_async_copy(normer, n0v, lsem.at[10]))
    loads.append(pltpu.make_async_copy(stab, m0v, lsem.at[11]))
    loads.append(pltpu.make_async_copy(cell.at[0], cv.at[0], lsem.at[12]))
    loads.append(pltpu.make_async_copy(cell.at[1], cv.at[1], lsem.at[13]))
    for load in loads:
        load.start()

    barrier = pltpu.get_barrier_semaphore()
    for t in tp_peers:
        pl.semaphore_signal(barrier, inc=1, device_id={"tp": t})
    for d in dp_peers:
        pl.semaphore_signal(barrier, inc=1, device_id={"dp": d})
    loads[0].wait()
    pl.semaphore_wait(barrier, TP + DP - 2)

    def send(src, dst, sem, axis, peer):
        pltpu.make_async_remote_copy(
            src_ref=src,
            dst_ref=dst,
            send_sem=ssem.at[sem],
            recv_sem=rsem.at[sem],
            device_id={axis: peer},
        ).start()

    def wait_bytes(ref, sem):
        pltpu.make_async_copy(ref, ref, sem).wait()

    def gather_rows(b, sem):
        for t in tp_peers:
            send(g.at[b, own_t], g.at[b, own_t], sem, "tp", t)

    gather_rows(0, 0)

    for load in loads[1:12]:
        load.wait()
    row = lax.broadcasted_iota(jnp.int32, (DH, TP), 0)
    col = lax.broadcasted_iota(jnp.int32, (DH, TP), 1)
    for b in range(NB):
        picked = jnp.zeros((DH, COLS), F32)
        for i in range(2):
            onehot = jnp.where((row == i) & (col == me_t), 1.0, 0.0).astype(BF16)
            picked = picked + jnp.dot(onehot, gates[i, b], preferred_element_type=F32)
        grow[b] = picked.astype(BF16)
    for b in range(NB):
        loads[12 + b].wait()

        def split(s, carry):
            c0 = cv[b, s]
            hi = c0.astype(BF16)
            chl[b, s, 0:DH] = hi
            chl[b, s, DH : 2 * DH] = (c0 - hi.astype(F32)).astype(BF16)
            return carry

        lax.fori_loop(0, DROWS, split, 0)

    lane = lax.broadcasted_iota(jnp.int32, (DROWS, DH), 1)
    eye = lax.broadcasted_iota(jnp.int32, (DROWS, DROWS), 0) == lax.broadcasted_iota(
        jnp.int32, (DROWS, DROWS), 1
    )
    sub8 = lax.broadcasted_iota(jnp.int32, (8, DH), 0)
    lane_q = lax.broadcasted_iota(jnp.int32, (DH, DROWS), 1)
    half = SIDE * DROWS
    stores = []
    outs = ((osend0, orecv0), (osend1, orecv1))

    for b in range(NB):
        base = SEMS * b
        wait_bytes(g.at[b, pl.ds(0, ROWS - TROWS)], rsem.at[base])

        for h, c in ((0, 1 - core), (1, core)):
            squares = []
            for yy in range(SIDE):
                rows = pl.ds(pl.multiple_of((2 * yy + c) * DROWS, DROWS), DROWS)
                xf = g[b, rows].astype(F32)
                squares.append(jnp.sum(xf * xf, axis=1, keepdims=True))
                scaled[h, yy * DROWS : (yy + 1) * DROWS] = (
                    xf * ngv[pl.ds(b, 1), :]
                ).astype(BF16)
            dst = (dsend, ysend)[h]
            for i in range(2):
                two = jnp.dot(
                    scaled[h],
                    w[b, :, 2 * i * DH : 2 * (i + 1) * DH],
                    preferred_element_type=F32,
                )
                for n in range(2):
                    dst[b, 2 * i + n] = two[:, n * DH : (n + 1) * DH].reshape(
                        SIDE, DROWS, DH
                    )
                    if h == 0:
                        at = base + 1 + 2 * i + n
                        src = dsend.at[b, 2 * i + n]
                        send(src, drecv.at[b, 2 * i + n], at, "dp", partner)
            tail = dot_nt(scaled[h], grow[b])
            for yy in range(SIDE):
                dst[b, 4, yy] = jnp.where(
                    lane == 2, squares[yy], tail[yy * DROWS : (yy + 1) * DROWS]
                )
            if h == 0:
                send(dsend.at[b, 4], drecv.at[b, 4], base + 5, "dp", partner)

        for i in (0, 1, 2, 4, 3):
            wait_bytes(drecv.at[b, i], rsem.at[base + 1 + i])
            ysend[b, i] = ysend[b, i] + drecv[b, i]
            for yy in y_peers:
                send(
                    ysend.at[b, i, yy],
                    yrecv.at[b, i, y],
                    base + 6 + i,
                    "dp",
                    yy * 2 + core,
                )

        def arrived(i):
            wait_bytes(yrecv.at[b, i, pl.ds(0, SIDE - 1)], rsem.at[base + 6 + i])
            total = ysend[b, i, y]
            for yy in y_peers:
                total = total + yrecv[b, i, yy]
            return total

        query = arrived(0)
        q_hi = query.astype(BF16).astype(F32)
        q_lo = query - q_hi
        groups = []
        for j in range(DROWS // 8):
            rows = slice(8 * j, 8 * j + 8)
            qs[j] = jnp.concatenate([q_hi[rows], q_lo[rows]], axis=0).astype(BF16)
        for j in range(DROWS // 8):
            acc = jnp.zeros((8, DH), F32)
            for i in range(8):
                r = dot_nt(qs[j], chl[b, 8 * j + i])
                r = r[0:8, 0:DH] + (r[8:16, 0:DH] + r[0:8, DH : 2 * DH])
                acc = jnp.where(sub8 == i, r, acc)
            groups.append(acc)
        old_read = jnp.concatenate(groups, axis=0)

        key = arrived(1)
        value = arrived(2)
        tail = arrived(4)
        inv_rms = lax.rsqrt(tail[:, 2:3] * (1.0 / D) + EPSILON)
        query = query * inv_rms
        old_read = old_read * inv_rms
        key = key * (inv_rms * DH**-0.5)
        value = value * inv_rms
        igate = tail[:, 0:1] * inv_rms
        fpre = tail[:, 1:2] * inv_rms
        forget = jnp.minimum(fpre, 0.0) - jnp.log1p(jnp.exp(-jnp.abs(fpre)))
        prev = jnp.sum(jnp.where(eye, m0v[pl.ds(b, 1), :], 0.0), axis=1, keepdims=True)
        new_stab = jnp.maximum(forget + prev, igate)
        keep = jnp.exp(forget + prev - new_stab)
        write = jnp.exp(igate - new_stab)
        new_normer = keep * n0v[b] + write * key
        key_query = jnp.sum(key * query, axis=1, keepdims=True)
        numer = keep * old_read + (write * key_query) * value
        denom = jnp.maximum(
            jnp.abs(jnp.sum(new_normer * query, axis=1, keepdims=True)), 1.0
        )
        readout = numer / denom
        normed = readout * lax.rsqrt(
            jnp.mean(readout * readout, axis=1, keepdims=True) + EPSILON
        )
        normed = normed * hgv[pl.ds(b, 1), :]
        outgate = arrived(3) * inv_rms
        gat[b, own_d] = (normed / (1.0 + jnp.exp(-outgate))).astype(BF16)
        for d in dp_peers:
            send(gat.at[b, own_d], gat.at[b, own_d], base + 11, "dp", d)

        n1v[b] = new_normer
        m1v[pl.ds(b, 1), :] = jnp.sum(
            jnp.where(eye, new_stab, 0.0), axis=0, keepdims=True
        )
        wvt[0:DROWS] = jnp.broadcast_to(keep, (DROWS, DH))
        wvt[DROWS : 2 * DROWS] = key
        wv_cols = jnp.transpose(write * value)

        def update(s, carry):
            column = jnp.sum(
                jnp.where(lane_q == s, wv_cols, 0.0), axis=1, keepdims=True
            )
            k_row = wvt[pl.ds(DROWS + s, 1), :]
            keep_row = wvt[pl.ds(s, 1), :]
            cv[b, s] = keep_row * cv[b, s] + column * k_row
            return carry

        lax.fori_loop(0, DROWS, update, 0)
        stores.append(pltpu.make_async_copy(cv.at[b], cell_out.at[b], wsem.at[b]))
        stores[-1].start()

        wait_bytes(gat.at[b, pl.ds(0, ROWS - DROWS)], rsem.at[base + 11])
        osend, orecv = outs[b]
        osend[...] = jnp.dot(gat[b], pwv[b], preferred_element_type=F32).astype(
            osend.dtype
        )
        for t in tp_peers:
            rows = pl.ds(pl.multiple_of(t * TROWS, TROWS), TROWS)
            send(osend.at[rows], orecv.at[me_t], base + 12, "tp", t)
        orecv[me_t] = osend[own_t]
        wait_bytes(orecv.at[pl.ds(0, TP - 1)], rsem.at[base + 12])
        rows_sum = orecv[0].astype(F32)
        for i in range(1, TP):
            rows_sum = rows_sum + orecv[i].astype(F32)
        if b + 1 < NB:
            g[b + 1, own_t] = rows_sum.astype(BF16)
            gather_rows(b + 1, base + SEMS)
        else:
            fin[...] = rows_sum.astype(BF16)

    for i, (src, dst) in enumerate(
        ((fin, final_out), (n1v, normer_out), (m1v, stab_out))
    ):
        stores.append(pltpu.make_async_copy(src, dst, wsem.at[NB + i]))
        stores[-1].start()
    for b in range(NB):
        base = SEMS * b
        wait_bytes(g.at[b, pl.ds(0, ROWS - TROWS)], ssem.at[base])
        for i in range(5):
            wait_bytes(drecv.at[b, i], ssem.at[base + 1 + i])
            wait_bytes(yrecv.at[b, i, pl.ds(0, SIDE - 1)], ssem.at[base + 6 + i])
        wait_bytes(gat.at[b, pl.ds(0, ROWS - DROWS)], ssem.at[base + 11])
        wait_bytes(outs[b][1].at[pl.ds(0, TP - 1)], ssem.at[base + 12])
    for store in stores:
        store.wait()


def hand_on(final, cell, normer, stab, final_out, cell_out, normer_out, stab_out, *rest):
    fin, cv, n1v, m1v, sem_in, sem_out = rest
    pairs = []
    for b in range(NB):
        for i in range(PIECES):
            rows = pl.ds(i * (DROWS // PIECES), DROWS // PIECES)
            pairs.append((cell.at[b, rows], cv.at[b, rows], cell_out.at[b, rows]))
    pairs.append((final, fin, final_out))
    pairs.append((normer, n1v, normer_out))
    pairs.append((stab, m1v, stab_out))
    reads = [
        pltpu.make_async_copy(src, mid, sem_in.at[i])
        for i, (src, mid, _) in enumerate(pairs)
    ]
    writes = [
        pltpu.make_async_copy(mid, dst, sem_out.at[i])
        for i, (_, mid, dst) in enumerate(pairs)
    ]
    for read in reads:
        read.start()
    for read, write in zip(reads, writes):
        read.wait()
        write.start()
    for write in writes:
        write.wait()


def per_device(
    tokens,
    query_weight,
    key_weight,
    value_weight,
    outgate_weight,
    igate_weight,
    fgate_weight,
    norm_gain,
    head_gain,
    proj_weight,
    cell_state,
    normer_state,
    stab_state,
):
    anywhere = pl.BlockSpec(memory_space=pl.ANY)
    results = (
        jax.ShapeDtypeStruct((TROWS, COLS), BF16),
        jax.ShapeDtypeStruct((NB, DROWS, DH, DH), F32),
        jax.ShapeDtypeStruct((NB, DROWS, DH), F32),
        jax.ShapeDtypeStruct((NB, DROWS), F32),
    )
    held = pl.pallas_call(
        mega,
        out_shape=results,
        in_specs=[anywhere] * 13,
        out_specs=(anywhere,) * 4,
        scratch_shapes=[
            pltpu.VMEM((NB, ROWS, COLS), BF16),
            pltpu.VMEM((NB, COLS, QKVO), BF16),
            pltpu.VMEM((2, NB, TP, COLS), BF16),
            pltpu.VMEM((NB, DH, COLS), BF16),
            pltpu.VMEM((NB, DH, COLS), BF16),
            pltpu.VMEM((NB, COLS), F32),
            pltpu.VMEM((NB, DH), F32),
            pltpu.VMEM((NB, DROWS, DH), F32),
            pltpu.VMEM((NB, DROWS), F32),
            pltpu.VMEM((NB, DROWS, DH, DH), F32),
            pltpu.VMEM((NB, DROWS, 2 * DH, DH), BF16),
            pltpu.VMEM((2, SIDE * DROWS, COLS), BF16),
            pltpu.VMEM((NB, 5, SIDE, DROWS, DH), F32),
            pltpu.VMEM((NB, 5, SIDE, DROWS, DH), F32),
            pltpu.VMEM((NB, 5, SIDE, DROWS, DH), F32),
            pltpu.VMEM((NB, 5, SIDE, DROWS, DH), F32),
            pltpu.VMEM((DROWS // 8, 16, DH), BF16),
            pltpu.VMEM((2 * DROWS, DH), F32),
            pltpu.VMEM((NB, ROWS, DH), BF16),
            pltpu.VMEM((ROWS, COLS), F32),
            pltpu.VMEM((ROWS, COLS), BF16),
            pltpu.VMEM((TP, TROWS, COLS), F32),
            pltpu.VMEM((TP, TROWS, COLS), BF16),
            pltpu.VMEM((TROWS, COLS), BF16),
            pltpu.VMEM((NB, DROWS, DH), F32),
            pltpu.VMEM((NB, DROWS), F32),
            pltpu.SemaphoreType.DMA((14,)),
            pltpu.SemaphoreType.DMA((NB + 3,)),
            pltpu.SemaphoreType.DMA((SEMS * NB,)),
            pltpu.SemaphoreType.DMA((SEMS * NB,)),
        ],
        compiler_params=pltpu.CompilerParams(
            collective_id=0, has_side_effects=True, vmem_limit_bytes=60 * 10**6
        ),
        name="two_blocks",
    )(
        tokens,
        query_weight,
        key_weight,
        value_weight,
        outgate_weight,
        jnp.swapaxes(igate_weight, 1, 2),
        jnp.swapaxes(fgate_weight, 1, 2),
        norm_gain,
        head_gain,
        proj_weight,
        cell_state.reshape(NB, DROWS, DH, DH),
        normer_state.reshape(NB, DROWS, DH),
        stab_state.reshape(NB, DROWS),
    )
    moves = NB * PIECES + 3
    final_rows, cells, normers, stabs = pl.pallas_call(
        hand_on,
        out_shape=results,
        in_specs=[anywhere] * 4,
        out_specs=(anywhere,) * 4,
        scratch_shapes=[pltpu.VMEM(r.shape, r.dtype) for r in results]
        + [pltpu.SemaphoreType.DMA((moves,)), pltpu.SemaphoreType.DMA((moves,))],
        compiler_params=pltpu.CompilerParams(vmem_limit_bytes=60 * 10**6),
        name="hand_on",
    )(*held)
    return (
        final_rows,
        cells.reshape(cell_state.shape),
        normers.reshape(normer_state.shape),
        stabs.reshape(stab_state.shape),
    )


def solution(mesh):
    return jax.shard_map(
        per_device,
        mesh=mesh,
        in_specs=(
            P("tp", "dp"),
            P(None, "dp", "tp"),
            P(None, "dp", "tp"),
            P(None, "dp", "tp"),
            P(None, "dp", "tp"),
            P(),
            P(),
            P(None, "dp"),
            P(None, "tp"),
            P(None, "tp", "dp"),
            P(None, "dp", "tp", None, None),
            P(None, "dp", "tp", None),
            P(None, "dp", "tp"),
        ),
        out_specs=(
            P("tp", "dp"),
            P(None, "dp", "tp", None, None),
            P(None, "dp", "tp", None),
            P(None, "dp", "tp"),
        ),
        check_vma=False,
    )
```

time: 129 us -> 61.1 us (0.47)
  Pallas kernels: 0 us -> 60.3 us
  waiting for transfers between devices: 35.1 us -> 0 us
  blocking collectives: 32 us -> 0 us
  starting transfers between devices: 29.1 us -> 0 us
  matrix products: 14.2 us -> 0 us
  other arithmetic: 9.01 us -> 0 us
  local copies, waits for them, and re-layouts: 7.31 us -> 0 us
    pallas_call x0 -> x2, Pallas kernels: none -> 60.3 us  [the longest x1 56.4 us: per_device(): pl.pallas_call(mega, out_shape=results, in_specs=[anywhere] * 13, out_spe...]
    all_to_all x5 -> x0, waiting for transfers between devices: 35.1 us -> none  [the longest x3 26.7 us: sum_at_owner(): lax.all_to_all(parts, axis, split_axis=0, concat_axis=0, tiled=True)]
    all_to_all x3 -> x0, blocking collectives: 32 us -> none  [the longest x2 18.8 us: from_everyone(): return lax.all_to_all(copies, axis, split_axis=0, concat_axis=0, tiled=True)]
    all_to_all x5 -> x0, starting transfers between devices: 29.1 us -> none  [the longest x3 16.5 us: sum_at_owner(): lax.all_to_all(parts, axis, split_axis=0, concat_axis=0, tiled=True)]
    dot_general x16 -> x0, matrix products: 14.2 us -> none  [the longest x2 10.2 us: per_device(): jnp.einsum('bhvd,bhd->bhv', new_cell, query_rows, precision=lax.Precision...]
    another operation x3 -> x0, other arithmetic: 3.47 us -> none  [the longest x1 2.28 us: per_device(): jnp.stack(cell_list)]
    add x1 -> x0, other arithmetic: 2.98 us -> none  [per_device(): keep_rate[..., None, None] * cell_state[layer_num]]
    slice x3 -> x0, local copies, waits for them, and re-layouts: 2.75 us -> none  [the longest x1 0.99 us: per_device(): igate_weight[layer_num]]
  transfers between devices with their start and end apart: 5 -> 0, of which waited for: 5 -> 0; matrix products, arithmetic and copies ran while one was open for 7% -> 0% of each run, Pallas kernels for 0% -> 0%
where the time goes in v1:
time: 61.1 us; the launch traced here: 60.9 us
  Pallas kernels  60.3 us (99%)
  between operations  0.64 us (1%)
    pallas_call x1, Pallas kernels, per_device(): pl.pallas_call(mega, out_shape=results, in_specs=[anywhere] * 13, out_spe...  56.4 us
    pallas_call x1, Pallas kernels, per_device(): pl.pallas_call(hand_on, out_shape=results, in_specs=[anywhere] * 4, out_s...  3.91 us

profile of v1, /device:TPU:1, one launch (start us, length us, event | category | flops | bytes accessed | tf_op | source)
XLA Modules:
  0.0 60.9 jit_solution(17632501595933050371)
XLA Ops:
  0.6 56.4 %two_blocks.1 = (bf16[16,512]{1,0:T(8,128)(2,1)}, f32[2,32,128,128]{3,2,1,0:T(8,128)}, f32[2,32,128]{2,1,0:T(8,128)}, f32[2,32]{1,0:T(2,128)}) custom-call(bf16[16,512]{1,0:T(8,128)(2,1)} %tok.1, bf16[2,512,128]{2,1,0:T(8,128)(2,1)} %qw.1, bf16[2,512,128]{2,1,0:T(8,128)(2,1)} %kw.1, bf16[2,512,128]{2,1,0:T(8,128)(2,1)} %vw.1, bf16[2,512,128]{2,1,0:T(8,128)(2,1)} %ow.1, ...), custom_call_target="tpu_custom_call" | custom-call | tf_op jit(solution)/shard_map/two_blocks/pallas_call | solution.py:391
  57.0 3.9 %hand_on.1 = (bf16[16,512]{1,0:T(8,128)(2,1)}, f32[2,32,128,128]{3,2,1,0:T(8,128)}, f32[2,32,128]{2,1,0:T(8,128)}, f32[2,32]{1,0:T(2,128)}) custom-call(bf16[16,512]{1,0:T(8,128)(2,1)} %get-tuple-element.12.final, f32[2,32,128,128]{3,2,1,0:T(8,128)} %get-tuple-element.13.cell, f32[2,32,128]{2,1,0:T(8,128)} %get-tuple-element.14.normer, ...), custom_call_target="tpu_custom_call" | custom-call | tf_op jit(solution)/shard_map/hand_on/pallas_call | solution.py:448

commit v2 on v1

--- a/solution.py
+++ b/solution.py
@@ -19,7 +19,14 @@
 TROWS = ROWS // TP
 DROWS = ROWS // DP
 QKVO = 4 * DH
-SEMS = 13
+HALF = ROWS // 2
+ROWS_SEM = 0
+CORE_SEM = 1
+CHIP_SEM = 6
+GATED_SEM = 11
+OUT_SEM = 15
+SEMS = 16
+ORDER = (0, 1, 4, 3, 2)
 PIECES = 8
 
 F32 = jnp.float32
@@ -78,6 +85,10 @@
     drecv,
     ysend,
     yrecv,
+    tsend,
+    trecv,
+    tysend,
+    tyrecv,
     qs,
     wvt,
     gat,
@@ -150,10 +161,10 @@
 
     for load in loads[1:12]:
         load.wait()
-    row = lax.broadcasted_iota(jnp.int32, (DH, TP), 0)
-    col = lax.broadcasted_iota(jnp.int32, (DH, TP), 1)
+    row = lax.broadcasted_iota(jnp.int32, (TP, TP), 0)
+    col = lax.broadcasted_iota(jnp.int32, (TP, TP), 1)
     for b in range(NB):
-        picked = jnp.zeros((DH, COLS), F32)
+        picked = jnp.zeros((TP, COLS), F32)
         for i in range(2):
             onehot = jnp.where((row == i) & (col == me_t), 1.0, 0.0).astype(BF16)
             picked = picked + jnp.dot(onehot, gates[i, b], preferred_element_type=F32)
@@ -170,66 +181,82 @@
 
         lax.fori_loop(0, DROWS, split, 0)
 
-    lane = lax.broadcasted_iota(jnp.int32, (DROWS, DH), 1)
     eye = lax.broadcasted_iota(jnp.int32, (DROWS, DROWS), 0) == lax.broadcasted_iota(
         jnp.int32, (DROWS, DROWS), 1
     )
+    eye_wide = lax.broadcasted_iota(jnp.int32, (HALF, HALF), 0) == lax.broadcasted_iota(
+        jnp.int32, (HALF, HALF), 1
+    )
+    own_lane = (
+        lax.broadcasted_iota(jnp.int32, (DROWS, HALF), 0) + y * DROWS
+    ) == lax.broadcasted_iota(jnp.int32, (DROWS, HALF), 1)
     sub8 = lax.broadcasted_iota(jnp.int32, (8, DH), 0)
     lane_q = lax.broadcasted_iota(jnp.int32, (DH, DROWS), 1)
-    half = SIDE * DROWS
     stores = []
     outs = ((osend0, orecv0), (osend1, orecv1))
 
     for b in range(NB):
         base = SEMS * b
-        wait_bytes(g.at[b, pl.ds(0, ROWS - TROWS)], rsem.at[base])
-
+        wait_bytes(g.at[b, pl.ds(0, ROWS - TROWS)], rsem.at[base + ROWS_SEM])
+
+        sums = []
         for h, c in ((0, 1 - core), (1, core)):
             squares = []
             for yy in range(SIDE):
                 rows = pl.ds(pl.multiple_of((2 * yy + c) * DROWS, DROWS), DROWS)
                 xf = g[b, rows].astype(F32)
                 squares.append(jnp.sum(xf * xf, axis=1, keepdims=True))
-                scaled[h, yy * DROWS : (yy + 1) * DROWS] = (
-                    xf * ngv[pl.ds(b, 1), :]
-                ).astype(BF16)
-            dst = (dsend, ysend)[h]
-            for i in range(2):
-                two = jnp.dot(
-                    scaled[h],
-                    w[b, :, 2 * i * DH : 2 * (i + 1) * DH],
-                    preferred_element_type=F32,
-                )
-                for n in range(2):
-                    dst[b, 2 * i + n] = two[:, n * DH : (n + 1) * DH].reshape(
-                        SIDE, DROWS, DH
-                    )
-                    if h == 0:
-                        at = base + 1 + 2 * i + n
-                        src = dsend.at[b, 2 * i + n]
-                        send(src, drecv.at[b, 2 * i + n], at, "dp", partner)
-            tail = dot_nt(scaled[h], grow[b])
-            for yy in range(SIDE):
-                dst[b, 4, yy] = jnp.where(
-                    lane == 2, squares[yy], tail[yy * DROWS : (yy + 1) * DROWS]
-                )
-            if h == 0:
-                send(dsend.at[b, 4], drecv.at[b, 4], base + 5, "dp", partner)
-
-        for i in (0, 1, 2, 4, 3):
-            wait_bytes(drecv.at[b, i], rsem.at[base + 1 + i])
-            ysend[b, i] = ysend[b, i] + drecv[b, i]
+                at = h * HALF + yy * DROWS
+                scaled[at : at + DROWS] = (xf * ngv[pl.ds(b, 1), :]).astype(BF16)
+            sums.append(jnp.concatenate(squares, axis=0))
+
+        def to_partner(i):
+            if i < 4:
+                src, dst = dsend.at[b, i], drecv.at[b, i]
+            else:
+                src, dst = tsend.at[b], trecv.at[b]
+            send(src, dst, base + CORE_SEM + i, "dp", partner)
+
+        def project(i):
+            two = jnp.dot(
+                scaled[...],
+                w[b, :, 2 * i * DH : 2 * (i + 1) * DH],
+                preferred_element_type=F32,
+            )
+            for n in range(2):
+                tile = two[:, n * DH : (n + 1) * DH]
+                dsend[b, 2 * i + n] = tile[0:HALF].reshape(SIDE, DROWS, DH)
+                ysend[b, 2 * i + n] = tile[HALF:].reshape(SIDE, DROWS, DH)
+
+        project(0)
+        to_partner(0)
+        to_partner(1)
+        tail = dot_nt(grow[b], scaled[...])
+        for h, dst in ((0, tsend), (1, tysend)):
+            row_sums = jnp.sum(jnp.where(eye_wide, sums[h], 0.0), axis=0, keepdims=True)
+            dst[b] = jnp.where(sub8 == 2, row_sums, tail[0:8, h * HALF : (h + 1) * HALF])
+        to_partner(4)
+        project(1)
+        to_partner(3)
+        to_partner(2)
+
+        for i in ORDER:
+            at = base + CHIP_SEM + i
+            if i < 4:
+                wait_bytes(drecv.at[b, i], rsem.at[base + CORE_SEM + i])
+                ysend[b, i] = ysend[b, i] + drecv[b, i]
+            else:
+                wait_bytes(trecv.at[b], rsem.at[base + CORE_SEM + i])
+                tysend[b] = tysend[b] + trecv[b]
             for yy in y_peers:
-                send(
-                    ysend.at[b, i, yy],
-                    yrecv.at[b, i, y],
-                    base + 6 + i,
-                    "dp",
-                    yy * 2 + core,
-                )
+                if i < 4:
+                    src, dst = ysend.at[b, i, yy], yrecv.at[b, i, y]
+                else:
+                    src, dst = tysend.at[b], tyrecv.at[b, y]
+                send(src, dst, at, "dp", yy * 2 + core)
 
         def arrived(i):
-            wait_bytes(yrecv.at[b, i, pl.ds(0, SIDE - 1)], rsem.at[base + 6 + i])
+            wait_bytes(yrecv.at[b, i, pl.ds(0, SIDE - 1)], rsem.at[base + CHIP_SEM + i])
             total = ysend[b, i, y]
             for yy in y_peers:
                 total = total + yrecv[b, i, yy]
@@ -252,15 +279,22 @@
         old_read = jnp.concatenate(groups, axis=0)
 
         key = arrived(1)
-        value = arrived(2)
-        tail = arrived(4)
-        inv_rms = lax.rsqrt(tail[:, 2:3] * (1.0 / D) + EPSILON)
+        wait_bytes(tyrecv.at[b, pl.ds(0, SIDE - 1)], rsem.at[base + CHIP_SEM + 4])
+        tail = tysend[b]
+        for yy in y_peers:
+            tail = tail + tyrecv[b, yy]
+
+        def column(i):
+            return jnp.sum(
+                jnp.where(own_lane, tail[i : i + 1], 0.0), axis=1, keepdims=True
+            )
+
+        inv_rms = lax.rsqrt(column(2) * (1.0 / D) + EPSILON)
         query = query * inv_rms
         old_read = old_read * inv_rms
         key = key * (inv_rms * DH**-0.5)
-        value = value * inv_rms
-        igate = tail[:, 0:1] * inv_rms
-        fpre = tail[:, 1:2] * inv_rms
+        igate = column(0) * inv_rms
+        fpre = column(1) * inv_rms
         forget = jnp.minimum(fpre, 0.0) - jnp.log1p(jnp.exp(-jnp.abs(fpre)))
         prev = jnp.sum(jnp.where(eye, m0v[pl.ds(b, 1), :], 0.0), axis=1, keepdims=True)
         new_stab = jnp.maximum(forget + prev, igate)
@@ -268,19 +302,43 @@
         write = jnp.exp(igate - new_stab)
         new_normer = keep * n0v[b] + write * key
         key_query = jnp.sum(key * query, axis=1, keepdims=True)
-        numer = keep * old_read + (write * key_query) * value
         denom = jnp.maximum(
             jnp.abs(jnp.sum(new_normer * query, axis=1, keepdims=True)), 1.0
         )
+        outgate = arrived(3) * inv_rms
+        scale = hgv[pl.ds(b, 1), :] / (1.0 + jnp.exp(-outgate))
+        value = arrived(2) * inv_rms
+        numer = keep * old_read + (write * key_query) * value
         readout = numer / denom
         normed = readout * lax.rsqrt(
             jnp.mean(readout * readout, axis=1, keepdims=True) + EPSILON
         )
-        normed = normed * hgv[pl.ds(b, 1), :]
-        outgate = arrived(3) * inv_rms
-        gat[b, own_d] = (normed / (1.0 + jnp.exp(-outgate))).astype(BF16)
-        for d in dp_peers:
-            send(gat.at[b, own_d], gat.at[b, own_d], base + 11, "dp", d)
+        gat[b, own_d] = (normed * scale).astype(BF16)
+        for dy, dc in DP_STEPS:
+            peer = ((y + dy) % SIDE) * 2 + (core + dc) % 2
+            at = base + GATED_SEM + (SIDE - dy) % SIDE
+            send(gat.at[b, own_d], gat.at[b, own_d], at, "dp", peer)
+
+        osend, orecv = outs[b]
+        for dy in (0, 1, 3, 2):
+            yy = (y + dy) % SIDE
+            pieces = gat.at[b, pl.ds(0, DROWS if dy == 0 else 2 * DROWS)]
+            wait_bytes(pieces, rsem.at[base + GATED_SEM + dy])
+            rows = pl.ds(pl.multiple_of(yy * 2 * DROWS, 2 * DROWS), 2 * DROWS)
+            osend[rows] = jnp.dot(
+                gat[b, rows], pwv[b], preferred_element_type=F32
+            ).astype(osend.dtype)
+
+            def give(t):
+                src = osend.at[pl.ds(pl.multiple_of(t * TROWS, TROWS), TROWS)]
+                send(src, orecv.at[me_t], base + OUT_SEM, "tp", t)
+
+            for dx in (2, 1, 3):
+                give(yy * SIDE + (x + dx) % SIDE)
+
+            @pl.when(yy != z)
+            def _():
+                give(yy * SIDE + x)
 
         n1v[b] = new_normer
         m1v[pl.ds(b, 1), :] = jnp.sum(
@@ -303,22 +361,14 @@
         stores.append(pltpu.make_async_copy(cv.at[b], cell_out.at[b], wsem.at[b]))
         stores[-1].start()
 
-        wait_bytes(gat.at[b, pl.ds(0, ROWS - DROWS)], rsem.at[base + 11])
-        osend, orecv = outs[b]
-        osend[...] = jnp.dot(gat[b], pwv[b], preferred_element_type=F32).astype(
-            osend.dtype
-        )
-        for t in tp_peers:
-            rows = pl.ds(pl.multiple_of(t * TROWS, TROWS), TROWS)
-            send(osend.at[rows], orecv.at[me_t], base + 12, "tp", t)
         orecv[me_t] = osend[own_t]
-        wait_bytes(orecv.at[pl.ds(0, TP - 1)], rsem.at[base + 12])
+        wait_bytes(orecv.at[pl.ds(0, TP - 1)], rsem.at[base + OUT_SEM])
         rows_sum = orecv[0].astype(F32)
         for i in range(1, TP):
             rows_sum = rows_sum + orecv[i].astype(F32)
         if b + 1 < NB:
             g[b + 1, own_t] = rows_sum.astype(BF16)
-            gather_rows(b + 1, base + SEMS)
+            gather_rows(b + 1, base + SEMS + ROWS_SEM)
         else:
             fin[...] = rows_sum.astype(BF16)
 
@@ -329,12 +379,17 @@
         stores[-1].start()
     for b in range(NB):
         base = SEMS * b
-        wait_bytes(g.at[b, pl.ds(0, ROWS - TROWS)], ssem.at[base])
-        for i in range(5):
-            wait_bytes(drecv.at[b, i], ssem.at[base + 1 + i])
-            wait_bytes(yrecv.at[b, i, pl.ds(0, SIDE - 1)], ssem.at[base + 6 + i])
-        wait_bytes(gat.at[b, pl.ds(0, ROWS - DROWS)], ssem.at[base + 11])
-        wait_bytes(outs[b][1].at[pl.ds(0, TP - 1)], ssem.at[base + 12])
+        wait_bytes(g.at[b, pl.ds(0, ROWS - TROWS)], ssem.at[base + ROWS_SEM])
+        for i in range(4):
+            wait_bytes(drecv.at[b, i], ssem.at[base + CORE_SEM + i])
+            pieces = yrecv.at[b, i, pl.ds(0, SIDE - 1)]
+            wait_bytes(pieces, ssem.at[base + CHIP_SEM + i])
+        wait_bytes(trecv.at[b], ssem.at[base + CORE_SEM + 4])
+        wait_bytes(tyrecv.at[b, pl.ds(0, SIDE - 1)], ssem.at[base + CHIP_SEM + 4])
+        for dy in range(SIDE):
+            pieces = gat.at[b, pl.ds(0, DROWS if dy == 0 else 2 * DROWS)]
+            wait_bytes(pieces, ssem.at[base + GATED_SEM + dy])
+        wait_bytes(outs[b][1].at[pl.ds(0, TP - 1)], ssem.at[base + OUT_SEM])
     for store in stores:
         store.wait()
 
@@ -397,7 +452,7 @@
             pltpu.VMEM((NB, ROWS, COLS), BF16),
             pltpu.VMEM((NB, COLS, QKVO), BF16),
             pltpu.VMEM((2, NB, TP, COLS), BF16),
-            pltpu.VMEM((NB, DH, COLS), BF16),
+            pltpu.VMEM((NB, TP, COLS), BF16),
             pltpu.VMEM((NB, DH, COLS), BF16),
             pltpu.VMEM((NB, COLS), F32),
             pltpu.VMEM((NB, DH), F32),
@@ -405,11 +460,15 @@
             pltpu.VMEM((NB, DROWS), F32),
             pltpu.VMEM((NB, DROWS, DH, DH), F32),
             pltpu.VMEM((NB, DROWS, 2 * DH, DH), BF16),
-            pltpu.VMEM((2, SIDE * DROWS, COLS), BF16),
-            pltpu.VMEM((NB, 5, SIDE, DROWS, DH), F32),
-            pltpu.VMEM((NB, 5, SIDE, DROWS, DH), F32),
-            pltpu.VMEM((NB, 5, SIDE, DROWS, DH), F32),
-            pltpu.VMEM((NB, 5, SIDE, DROWS, DH), F32),
+            pltpu.VMEM((ROWS, COLS), BF16),
+            pltpu.VMEM((NB, 4, SIDE, DROWS, DH), F32),
+            pltpu.VMEM((NB, 4, SIDE, DROWS, DH), F32),
+            pltpu.VMEM((NB, 4, SIDE, DROWS, DH), F32),
+            pltpu.VMEM((NB, 4, SIDE, DROWS, DH), F32),
+            pltpu.VMEM((NB, 8, HALF), F32),
+            pltpu.VMEM((NB, 8, HALF), F32),
+            pltpu.VMEM((NB, 8, HALF), F32),
+            pltpu.VMEM((NB, SIDE, 8, HALF), F32),
             pltpu.VMEM((DROWS // 8, 16, DH), BF16),
             pltpu.VMEM((2 * DROWS, DH), F32),
             pltpu.VMEM((NB, ROWS, DH), BF16),

time: 61.1 us -> 61.2 us (level)
  no operation moved by 1% of the time
where the time goes in v2:
time: 61.2 us; the launch traced here: 60.4 us
  Pallas kernels  59.8 us (98%)
  between operations  0.64 us (1%)
    pallas_call x1, Pallas kernels, per_device(): pl.pallas_call(mega, out_shape=results, in_specs=[anywhere] * 13, out_spe...  55.9 us
    pallas_call x1, Pallas kernels, per_device(): pl.pallas_call(hand_on, out_shape=results, in_specs=[anywhere] * 4, out_s...  3.91 us

profile of v2, /device:TPU:1, one launch (start us, length us, event | category | flops | bytes accessed | tf_op | source)
XLA Modules:
  0.0 60.4 jit_solution(4366900315975753485)
XLA Ops:
  0.6 55.9 %two_blocks.1 = (bf16[16,512]{1,0:T(8,128)(2,1)}, f32[2,32,128,128]{3,2,1,0:T(8,128)}, f32[2,32,128]{2,1,0:T(8,128)}, f32[2,32]{1,0:T(2,128)}) custom-call(bf16[16,512]{1,0:T(8,128)(2,1)} %tok.1, bf16[2,512,128]{2,1,0:T(8,128)(2,1)} %qw.1, bf16[2,512,128]{2,1,0:T(8,128)(2,1)} %kw.1, bf16[2,512,128]{2,1,0:T(8,128)(2,1)} %vw.1, bf16[2,512,128]{2,1,0:T(8,128)(2,1)} %ow.1, ...), custom_call_target="tpu_custom_call" | custom-call | tf_op jit(solution)/shard_map/two_blocks/pallas_call | solution.py:446
  56.5 3.9 %hand_on.1 = (bf16[16,512]{1,0:T(8,128)(2,1)}, f32[2,32,128,128]{3,2,1,0:T(8,128)}, f32[2,32,128]{2,1,0:T(8,128)}, f32[2,32]{1,0:T(2,128)}) custom-call(bf16[16,512]{1,0:T(8,128)(2,1)} %get-tuple-element.12.final, f32[2,32,128,128]{3,2,1,0:T(8,128)} %get-tuple-element.13.cell, f32[2,32,128]{2,1,0:T(8,128)} %get-tuple-element.14.normer, ...), custom_call_target="tpu_custom_call" | custom-call | tf_op jit(solution)/shard_map/hand_on/pallas_call | solution.py:507

commit v3 on v1

--- a/solution.py
+++ b/solution.py
@@ -19,7 +19,17 @@
 TROWS = ROWS // TP
 DROWS = ROWS // DP
 QKVO = 4 * DH
-SEMS = 13
+ROWS_SEM = 0
+CORE_SEM = 4
+CHIP_SEM = 8
+GATED_SEM = 13
+OUT_SEM = 17
+SEMS = 18
+ORDER = (0, 1, 4, 3, 2)
+TILES = [(i * 32, 32) for i in range(4)] + [(128, 8)]
+TALL = 136
+GROUP = 64
+NEAR_FIRST = (0, 1, 3, 2)
 PIECES = 8
 
 F32 = jnp.float32
@@ -73,10 +83,8 @@
     m0v,
     cv,
     chl,
-    scaled,
-    dsend,
+    part,
     drecv,
-    ysend,
     yrecv,
     qs,
     wvt,
@@ -99,7 +107,6 @@
     y, core = me_d // 2, me_d % 2
     tp_peers = [((z + dz) % SIDE) * SIDE + (x + dx) % SIDE for dz, dx in TP_STEPS]
     dp_peers = [((y + dy) % SIDE) * 2 + (core + dc) % 2 for dy, dc in DP_STEPS]
-    y_peers = [(y + dy) % SIDE for dy in (2, 1, 3)]
     partner = y * 2 + 1 - core
     own_t = pl.ds(pl.multiple_of(me_t * TROWS, TROWS), TROWS)
     own_d = pl.ds(pl.multiple_of(me_d * DROWS, DROWS), DROWS)
@@ -142,23 +149,25 @@
     def wait_bytes(ref, sem):
         pltpu.make_async_copy(ref, ref, sem).wait()
 
-    def gather_rows(b, sem):
-        for t in tp_peers:
-            send(g.at[b, own_t], g.at[b, own_t], sem, "tp", t)
-
-    gather_rows(0, 0)
+    def gather_rows(b):
+        for (dz, _), t in zip(TP_STEPS, tp_peers):
+            at = SEMS * b + ROWS_SEM + (SIDE - dz) % SIDE
+            send(g.at[b, own_t], g.at[b, own_t], at, "tp", t)
+
+    gather_rows(0)
 
     for load in loads[1:12]:
         load.wait()
-    row = lax.broadcasted_iota(jnp.int32, (DH, TP), 0)
-    col = lax.broadcasted_iota(jnp.int32, (DH, TP), 1)
+    row = lax.broadcasted_iota(jnp.int32, (TP, TP), 0)
+    col = lax.broadcasted_iota(jnp.int32, (TP, TP), 1)
     for b in range(NB):
-        picked = jnp.zeros((DH, COLS), F32)
+        picked = jnp.zeros((TP, COLS), F32)
         for i in range(2):
             onehot = jnp.where((row == i) & (col == me_t), 1.0, 0.0).astype(BF16)
             picked = picked + jnp.dot(onehot, gates[i, b], preferred_element_type=F32)
         grow[b] = picked.astype(BF16)
-    for b in range(NB):
+
+    def split_cells(b):
         loads[12 + b].wait()
 
         def split(s, carry):
@@ -170,69 +179,81 @@
 
         lax.fori_loop(0, DROWS, split, 0)
 
-    lane = lax.broadcasted_iota(jnp.int32, (DROWS, DH), 1)
     eye = lax.broadcasted_iota(jnp.int32, (DROWS, DROWS), 0) == lax.broadcasted_iota(
         jnp.int32, (DROWS, DROWS), 1
     )
+    eye_wide = lax.broadcasted_iota(
+        jnp.int32, (GROUP, GROUP), 0
+    ) == lax.broadcasted_iota(jnp.int32, (GROUP, GROUP), 1)
+    own_lane = (
+        lax.broadcasted_iota(jnp.int32, (DROWS, DH), 0) + core * DROWS
+    ) == lax.broadcasted_iota(jnp.int32, (DROWS, DH), 1)
+    sub8_group = lax.broadcasted_iota(jnp.int32, (8, GROUP), 0)
     sub8 = lax.broadcasted_iota(jnp.int32, (8, DH), 0)
     lane_q = lax.broadcasted_iota(jnp.int32, (DH, DROWS), 1)
-    half = SIDE * DROWS
     stores = []
     outs = ((osend0, orecv0), (osend1, orecv1))
 
     for b in range(NB):
         base = SEMS * b
-        wait_bytes(g.at[b, pl.ds(0, ROWS - TROWS)], rsem.at[base])
-
-        for h, c in ((0, 1 - core), (1, core)):
-            squares = []
-            for yy in range(SIDE):
-                rows = pl.ds(pl.multiple_of((2 * yy + c) * DROWS, DROWS), DROWS)
-                xf = g[b, rows].astype(F32)
-                squares.append(jnp.sum(xf * xf, axis=1, keepdims=True))
-                scaled[h, yy * DROWS : (yy + 1) * DROWS] = (
-                    xf * ngv[pl.ds(b, 1), :]
-                ).astype(BF16)
-            dst = (dsend, ysend)[h]
+
+        def project(k):
+            dz = NEAR_FIRST[k]
+            zz = (z + dz) % SIDE
+            count = 3 if dz == 0 else 4
+            wait_bytes(g.at[b, pl.ds(0, count * TROWS)], rsem.at[base + ROWS_SEM + dz])
+            xf = g[b, pl.ds(pl.multiple_of(zz * GROUP, GROUP), GROUP)].astype(F32)
+            squares = jnp.sum(xf * xf, axis=1, keepdims=True)
+            scaled = (xf * ngv[pl.ds(b, 1), :]).astype(BF16)
             for i in range(2):
                 two = jnp.dot(
-                    scaled[h],
+                    scaled,
                     w[b, :, 2 * i * DH : 2 * (i + 1) * DH],
                     preferred_element_type=F32,
                 )
                 for n in range(2):
-                    dst[b, 2 * i + n] = two[:, n * DH : (n + 1) * DH].reshape(
-                        SIDE, DROWS, DH
-                    )
-                    if h == 0:
-                        at = base + 1 + 2 * i + n
-                        src = dsend.at[b, 2 * i + n]
-                        send(src, drecv.at[b, 2 * i + n], at, "dp", partner)
-            tail = dot_nt(scaled[h], grow[b])
-            for yy in range(SIDE):
-                dst[b, 4, yy] = jnp.where(
-                    lane == 2, squares[yy], tail[yy * DROWS : (yy + 1) * DROWS]
-                )
-            if h == 0:
-                send(dsend.at[b, 4], drecv.at[b, 4], base + 5, "dp", partner)
-
-        for i in (0, 1, 2, 4, 3):
-            wait_bytes(drecv.at[b, i], rsem.at[base + 1 + i])
-            ysend[b, i] = ysend[b, i] + drecv[b, i]
-            for yy in y_peers:
-                send(
-                    ysend.at[b, i, yy],
-                    yrecv.at[b, i, y],
-                    base + 6 + i,
-                    "dp",
-                    yy * 2 + core,
-                )
+                    at, size = TILES[2 * i + n]
+                    for c in range(2):
+                        part[b, zz, c, at : at + size] = two[
+                            c * DROWS : (c + 1) * DROWS, n * DH : (n + 1) * DH
+                        ]
+            tail = dot_nt(grow[b], scaled)
+            sq_row = jnp.sum(jnp.where(eye_wide, squares, 0.0), axis=0, keepdims=True)
+            tail = jnp.where(sub8_group == 2, sq_row, tail[0:8])
+            tail = jnp.concatenate([tail, jnp.zeros_like(tail)], axis=1)
+            for c in range(2):
+                part[b, zz, c, 4 * DROWS : TALL] = tail
+            sem = base + CORE_SEM + k
+            send(part.at[b, zz, 1 - core], drecv.at[b, zz], sem, "dp", partner)
+
+        def pass_on(k):
+            zz = (z + NEAR_FIRST[k]) % SIDE
+            wait_bytes(drecv.at[b, zz], rsem.at[base + CORE_SEM + k])
+            part[b, zz, core] = part[b, zz, core] + drecv[b, zz]
+
+            @pl.when(zz != y)
+            def _():
+                for i in ORDER:
+                    rows = pl.ds(*TILES[i])
+                    src, dst = part.at[b, zz, core, rows], yrecv.at[b, y, rows]
+                    send(src, dst, base + CHIP_SEM + i, "dp", zz * 2 + core)
+
+        for k in range(SIDE):
+            project(k)
+            if k > 0:
+                pass_on(k - 1)
+        pass_on(SIDE - 1)
+        if b == 0:
+            split_cells(0)
 
         def arrived(i):
-            wait_bytes(yrecv.at[b, i, pl.ds(0, SIDE - 1)], rsem.at[base + 6 + i])
-            total = ysend[b, i, y]
-            for yy in y_peers:
-                total = total + yrecv[b, i, yy]
+            at, size = TILES[i]
+            wait_bytes(
+                yrecv.at[b, 0, pl.ds(0, 3 * size)], rsem.at[base + CHIP_SEM + i]
+            )
+            total = part[b, y, core, at : at + size]
+            for dy in range(1, SIDE):
+                total = total + yrecv[b, (y + dy) % SIDE, at : at + size]
             return total
 
         query = arrived(0)
@@ -252,15 +273,19 @@
         old_read = jnp.concatenate(groups, axis=0)
 
         key = arrived(1)
-        value = arrived(2)
         tail = arrived(4)
-        inv_rms = lax.rsqrt(tail[:, 2:3] * (1.0 / D) + EPSILON)
+
+        def column(i):
+            return jnp.sum(
+                jnp.where(own_lane, tail[i : i + 1], 0.0), axis=1, keepdims=True
+            )
+
+        inv_rms = lax.rsqrt(column(2) * (1.0 / D) + EPSILON)
         query = query * inv_rms
         old_read = old_read * inv_rms
         key = key * (inv_rms * DH**-0.5)
-        value = value * inv_rms
-        igate = tail[:, 0:1] * inv_rms
-        fpre = tail[:, 1:2] * inv_rms
+        igate = column(0) * inv_rms
+        fpre = column(1) * inv_rms
         forget = jnp.minimum(fpre, 0.0) - jnp.log1p(jnp.exp(-jnp.abs(fpre)))
         prev = jnp.sum(jnp.where(eye, m0v[pl.ds(b, 1), :], 0.0), axis=1, keepdims=True)
         new_stab = jnp.maximum(forget + prev, igate)
@@ -268,19 +293,43 @@
         write = jnp.exp(igate - new_stab)
         new_normer = keep * n0v[b] + write * key
         key_query = jnp.sum(key * query, axis=1, keepdims=True)
-        numer = keep * old_read + (write * key_query) * value
         denom = jnp.maximum(
             jnp.abs(jnp.sum(new_normer * query, axis=1, keepdims=True)), 1.0
         )
+        outgate = arrived(3) * inv_rms
+        scale = hgv[pl.ds(b, 1), :] / (1.0 + jnp.exp(-outgate))
+        value = arrived(2) * inv_rms
+        numer = keep * old_read + (write * key_query) * value
         readout = numer / denom
         normed = readout * lax.rsqrt(
             jnp.mean(readout * readout, axis=1, keepdims=True) + EPSILON
         )
-        normed = normed * hgv[pl.ds(b, 1), :]
-        outgate = arrived(3) * inv_rms
-        gat[b, own_d] = (normed / (1.0 + jnp.exp(-outgate))).astype(BF16)
+        gat[b, own_d] = (normed * scale).astype(BF16)
         for d in dp_peers:
-            send(gat.at[b, own_d], gat.at[b, own_d], base + 11, "dp", d)
+            send(gat.at[b, own_d], gat.at[b, own_d], base + GATED_SEM + y, "dp", d)
+
+        osend, orecv = outs[b]
+        for dz in NEAR_FIRST:
+            yy = (z + dz) % SIDE
+
+            @pl.when(yy == y)
+            def _():
+                wait_bytes(gat.at[b, pl.ds(0, DROWS)], rsem.at[base + GATED_SEM + yy])
+
+            @pl.when(yy != y)
+            def _():
+                wait_bytes(gat.at[b, pl.ds(0, GROUP)], rsem.at[base + GATED_SEM + yy])
+
+            rows = pl.ds(pl.multiple_of(yy * GROUP, GROUP), GROUP)
+            osend[rows] = jnp.dot(
+                gat[b, rows], pwv[b], preferred_element_type=F32
+            ).astype(osend.dtype)
+            for dx in (2, 1, 3, 0):
+                if (dz, dx) == (0, 0):
+                    continue
+                t = yy * SIDE + (x + dx) % SIDE
+                src = osend.at[pl.ds(pl.multiple_of(t * TROWS, TROWS), TROWS)]
+                send(src, orecv.at[me_t], base + OUT_SEM, "tp", t)
 
         n1v[b] = new_normer
         m1v[pl.ds(b, 1), :] = jnp.sum(
@@ -302,23 +351,17 @@
         lax.fori_loop(0, DROWS, update, 0)
         stores.append(pltpu.make_async_copy(cv.at[b], cell_out.at[b], wsem.at[b]))
         stores[-1].start()
-
-        wait_bytes(gat.at[b, pl.ds(0, ROWS - DROWS)], rsem.at[base + 11])
-        osend, orecv = outs[b]
-        osend[...] = jnp.dot(gat[b], pwv[b], preferred_element_type=F32).astype(
-            osend.dtype
-        )
-        for t in tp_peers:
-            rows = pl.ds(pl.multiple_of(t * TROWS, TROWS), TROWS)
-            send(osend.at[rows], orecv.at[me_t], base + 12, "tp", t)
+        if b == 0:
+            split_cells(1)
+
         orecv[me_t] = osend[own_t]
-        wait_bytes(orecv.at[pl.ds(0, TP - 1)], rsem.at[base + 12])
+        wait_bytes(orecv.at[pl.ds(0, TP - 1)], rsem.at[base + OUT_SEM])
         rows_sum = orecv[0].astype(F32)
         for i in range(1, TP):
             rows_sum = rows_sum + orecv[i].astype(F32)
         if b + 1 < NB:
             g[b + 1, own_t] = rows_sum.astype(BF16)
-            gather_rows(b + 1, base + SEMS)
+            gather_rows(b + 1)
         else:
             fin[...] = rows_sum.astype(BF16)
 
@@ -329,12 +372,16 @@
         stores[-1].start()
     for b in range(NB):
         base = SEMS * b
-        wait_bytes(g.at[b, pl.ds(0, ROWS - TROWS)], ssem.at[base])
+        for k in range(SIDE):
+            count = 3 if k == 0 else 4
+            wait_bytes(g.at[b, pl.ds(0, count * TROWS)], ssem.at[base + ROWS_SEM + k])
+            wait_bytes(drecv.at[b, k], ssem.at[base + CORE_SEM + k])
         for i in range(5):
-            wait_bytes(drecv.at[b, i], ssem.at[base + 1 + i])
-            wait_bytes(yrecv.at[b, i, pl.ds(0, SIDE - 1)], ssem.at[base + 6 + i])
-        wait_bytes(gat.at[b, pl.ds(0, ROWS - DROWS)], ssem.at[base + 11])
-        wait_bytes(outs[b][1].at[pl.ds(0, TP - 1)], ssem.at[base + 12])
+            pieces = yrecv.at[b, 0, pl.ds(0, 3 * TILES[i][1])]
+            wait_bytes(pieces, ssem.at[base + CHIP_SEM + i])
+        pieces = gat.at[b, pl.ds(0, (DP - 1) * DROWS)]
+        wait_bytes(pieces, ssem.at[base + GATED_SEM + y])
+        wait_bytes(outs[b][1].at[pl.ds(0, TP - 1)], ssem.at[base + OUT_SEM])
     for store in stores:
         store.wait()
 
@@ -397,7 +444,7 @@
             pltpu.VMEM((NB, ROWS, COLS), BF16),
             pltpu.VMEM((NB, COLS, QKVO), BF16),
             pltpu.VMEM((2, NB, TP, COLS), BF16),
-            pltpu.VMEM((NB, DH, COLS), BF16),
+            pltpu.VMEM((NB, TP, COLS), BF16),
             pltpu.VMEM((NB, DH, COLS), BF16),
             pltpu.VMEM((NB, COLS), F32),
             pltpu.VMEM((NB, DH), F32),
@@ -405,11 +452,9 @@
             pltpu.VMEM((NB, DROWS), F32),
             pltpu.VMEM((NB, DROWS, DH, DH), F32),
             pltpu.VMEM((NB, DROWS, 2 * DH, DH), BF16),
-            pltpu.VMEM((2, SIDE * DROWS, COLS), BF16),
-            pltpu.VMEM((NB, 5, SIDE, DROWS, DH), F32),
-            pltpu.VMEM((NB, 5, SIDE, DROWS, DH), F32),
-            pltpu.VMEM((NB, 5, SIDE, DROWS, DH), F32),
-            pltpu.VMEM((NB, 5, SIDE, DROWS, DH), F32),
+            pltpu.VMEM((NB, SIDE, 2, TALL, DH), F32),
+            pltpu.VMEM((NB, SIDE, TALL, DH), F32),
+            pltpu.VMEM((NB, SIDE, TALL, DH), F32),
             pltpu.VMEM((DROWS // 8, 16, DH), BF16),
             pltpu.VMEM((2 * DROWS, DH), F32),
             pltpu.VMEM((NB, ROWS, DH), BF16),

time: 61.1 us -> 59.2 us (0.969)
  Pallas kernels: 60.3 us -> 58.4 us
    pallas_call x1, Pallas kernels: 56.4 us -> 54.5 us  [per_device(): pl.pallas_call(mega, out_shape=results, in_specs=[anywhere] * 13, out_spe...]
where the time goes in v3:
time: 59.2 us; the launch traced here: 59.1 us
  Pallas kernels  58.4 us (99%)
  between operations  0.64 us (1%)
    pallas_call x1, Pallas kernels, per_device(): pl.pallas_call(mega, out_shape=results, in_specs=[anywhere] * 13, out_spe...  54.5 us
    pallas_call x1, Pallas kernels, per_device(): pl.pallas_call(hand_on, out_shape=results, in_specs=[anywhere] * 4, out_s...  3.91 us

profile of v3, /device:TPU:1, one launch (start us, length us, event | category | flops | bytes accessed | tf_op | source)
XLA Modules:
  0.0 59.1 jit_solution(4279424190871246835)
XLA Ops:
  0.6 54.5 %two_blocks.1 = (bf16[16,512]{1,0:T(8,128)(2,1)}, f32[2,32,128,128]{3,2,1,0:T(8,128)}, f32[2,32,128]{2,1,0:T(8,128)}, f32[2,32]{1,0:T(2,128)}) custom-call(bf16[16,512]{1,0:T(8,128)(2,1)} %tok.1, bf16[2,512,128]{2,1,0:T(8,128)(2,1)} %qw.1, bf16[2,512,128]{2,1,0:T(8,128)(2,1)} %kw.1, bf16[2,512,128]{2,1,0:T(8,128)(2,1)} %vw.1, bf16[2,512,128]{2,1,0:T(8,128)(2,1)} %ow.1, ...), custom_call_target="tpu_custom_call" | custom-call | tf_op jit(solution)/shard_map/two_blocks/pallas_call | solution.py:438
  55.2 3.9 %hand_on.1 = (bf16[16,512]{1,0:T(8,128)(2,1)}, f32[2,32,128,128]{3,2,1,0:T(8,128)}, f32[2,32,128]{2,1,0:T(8,128)}, f32[2,32]{1,0:T(2,128)}) custom-call(bf16[16,512]{1,0:T(8,128)(2,1)} %get-tuple-element.12.final, f32[2,32,128,128]{3,2,1,0:T(8,128)} %get-tuple-element.13.cell, f32[2,32,128]{2,1,0:T(8,128)} %get-tuple-element.14.normer, ...), custom_call_target="tpu_custom_call" | custom-call | tf_op jit(solution)/shard_map/hand_on/pallas_call | solution.py:493

commit v4 on v3

--- a/solution.py
+++ b/solution.py
@@ -24,7 +24,8 @@
 CHIP_SEM = 8
 GATED_SEM = 13
 OUT_SEM = 17
-SEMS = 18
+WEIGHT_SEM = 18
+SEMS = 19
 ORDER = (0, 1, 4, 3, 2)
 TILES = [(i * 32, 32) for i in range(4)] + [(128, 8)]
 TALL = 136
@@ -42,7 +43,7 @@
 
 TP_STEPS = sorted(
     ((dz, dx) for dz in range(SIDE) for dx in range(SIDE) if (dz, dx) != (0, 0)),
-    key=lambda s: -(ring_distance(s[0]) + ring_distance(s[1])),
+    key=lambda s: (-ring_distance(s[0]), -ring_distance(s[1])),
 )
 DP_STEPS = sorted(
     ((dy, dc) for dy in range(SIDE) for dc in range(2) if (dy, dc) != (0, 0)),
@@ -88,11 +89,10 @@
     yrecv,
     qs,
     wvt,
+    gsend,
     gat,
-    osend0,
-    osend1,
-    orecv0,
-    orecv1,
+    osend,
+    orecv,
     fin,
     n1v,
     m1v,
@@ -109,7 +109,6 @@
     dp_peers = [((y + dy) % SIDE) * 2 + (core + dc) % 2 for dy, dc in DP_STEPS]
     partner = y * 2 + 1 - core
     own_t = pl.ds(pl.multiple_of(me_t * TROWS, TROWS), TROWS)
-    own_d = pl.ds(pl.multiple_of(me_d * DROWS, DROWS), DROWS)
     own_cols = pl.ds(pl.multiple_of(me_d * COLS, COLS), COLS)
 
     loads = [pltpu.make_async_copy(tok, g.at[0, own_t], lsem.at[0])]
@@ -120,20 +119,21 @@
         loads.append(
             pltpu.make_async_copy(src, w.at[:, :, pl.ds(i * DH, DH)], lsem.at[4 + i])
         )
-    loads.append(pltpu.make_async_copy(pw, pwv, lsem.at[8]))
+    loads.append(pltpu.make_async_copy(pw.at[0], pwv.at[0, z], lsem.at[8]))
     loads.append(pltpu.make_async_copy(hgain, hgv, lsem.at[9]))
     loads.append(pltpu.make_async_copy(normer, n0v, lsem.at[10]))
     loads.append(pltpu.make_async_copy(stab, m0v, lsem.at[11]))
+    loads.append(pltpu.make_async_copy(pw.at[1], pwv.at[1, z], lsem.at[14]))
     loads.append(pltpu.make_async_copy(cell.at[0], cv.at[0], lsem.at[12]))
     loads.append(pltpu.make_async_copy(cell.at[1], cv.at[1], lsem.at[13]))
-    for load in loads:
-        load.start()
-
+    loads[0].start()
     barrier = pltpu.get_barrier_semaphore()
     for t in tp_peers:
         pl.semaphore_signal(barrier, inc=1, device_id={"tp": t})
     for d in dp_peers:
         pl.semaphore_signal(barrier, inc=1, device_id={"dp": d})
+    for load in loads[1:]:
+        load.start()
     loads[0].wait()
     pl.semaphore_wait(barrier, TP + DP - 2)
 
@@ -156,7 +156,7 @@
 
     gather_rows(0)
 
-    for load in loads[1:12]:
+    for load in loads[1:13]:
         load.wait()
     row = lax.broadcasted_iota(jnp.int32, (TP, TP), 0)
     col = lax.broadcasted_iota(jnp.int32, (TP, TP), 1)
@@ -168,7 +168,7 @@
         grow[b] = picked.astype(BF16)
 
     def split_cells(b):
-        loads[12 + b].wait()
+        loads[13 + b].wait()
 
         def split(s, carry):
             c0 = cv[b, s]
@@ -192,7 +192,6 @@
     sub8 = lax.broadcasted_iota(jnp.int32, (8, DH), 0)
     lane_q = lax.broadcasted_iota(jnp.int32, (DH, DROWS), 1)
     stores = []
-    outs = ((osend0, orecv0), (osend1, orecv1))
 
     for b in range(NB):
         base = SEMS * b
@@ -242,6 +241,9 @@
             project(k)
             if k > 0:
                 pass_on(k - 1)
+        for dz in (2, 1, 3):
+            t = (z + dz) % SIDE * SIDE + x
+            send(pwv.at[b, z], pwv.at[b, z], base + WEIGHT_SEM, "tp", t)
         pass_on(SIDE - 1)
         if b == 0:
             split_cells(0)
@@ -304,32 +306,30 @@
         normed = readout * lax.rsqrt(
             jnp.mean(readout * readout, axis=1, keepdims=True) + EPSILON
         )
-        gat[b, own_d] = (normed * scale).astype(BF16)
-        for d in dp_peers:
-            send(gat.at[b, own_d], gat.at[b, own_d], base + GATED_SEM + y, "dp", d)
-
-        osend, orecv = outs[b]
-        for dz in NEAR_FIRST:
-            yy = (z + dz) % SIDE
-
-            @pl.when(yy == y)
-            def _():
-                wait_bytes(gat.at[b, pl.ds(0, DROWS)], rsem.at[base + GATED_SEM + yy])
-
-            @pl.when(yy != y)
-            def _():
-                wait_bytes(gat.at[b, pl.ds(0, GROUP)], rsem.at[base + GATED_SEM + yy])
-
-            rows = pl.ds(pl.multiple_of(yy * GROUP, GROUP), GROUP)
-            osend[rows] = jnp.dot(
-                gat[b, rows], pwv[b], preferred_element_type=F32
-            ).astype(osend.dtype)
-            for dx in (2, 1, 3, 0):
-                if (dz, dx) == (0, 0):
-                    continue
-                t = yy * SIDE + (x + dx) % SIDE
-                src = osend.at[pl.ds(pl.multiple_of(t * TROWS, TROWS), TROWS)]
-                send(src, orecv.at[me_t], base + OUT_SEM, "tp", t)
+        gsend[b] = (normed * scale).astype(BF16)
+
+        def give_gated(dy, dc):
+            pltpu.make_async_remote_copy(
+                src_ref=gsend.at[b],
+                dst_ref=gat.at[b, 2 * z + core],
+                send_sem=ssem.at[base + GATED_SEM],
+                recv_sem=rsem.at[base + GATED_SEM + (z - y + SIDE) % SIDE],
+                device_id={
+                    "tp": y * SIDE + x,
+                    "dp": (y + dy) % SIDE * 2 + (core + dc) % 2,
+                },
+            ).start()
+
+        for dy, dc in DP_STEPS:
+            give_gated(dy, dc)
+
+        @pl.when(y != z)
+        def _():
+            give_gated(0, 0)
+
+        @pl.when(y == z)
+        def _():
+            gat[b, 2 * z + core] = gsend[b]
 
         n1v[b] = new_normer
         m1v[pl.ds(b, 1), :] = jnp.sum(
@@ -351,14 +351,42 @@
         lax.fori_loop(0, DROWS, update, 0)
         stores.append(pltpu.make_async_copy(cv.at[b], cell_out.at[b], wsem.at[b]))
         stores[-1].start()
+        for dz in NEAR_FIRST:
+            zz = (z + dz) % SIDE
+            at = rsem.at[base + GATED_SEM + dz]
+            if dz == 0:
+
+                @pl.when(y == z)
+                def _():
+                    wait_bytes(gat.at[b, pl.ds(0, 1)], at)
+
+                @pl.when(y != z)
+                def _():
+                    wait_bytes(gat.at[b, pl.ds(0, 2)], at)
+
+                partial = jnp.zeros((GROUP, COLS), F32)
+            else:
+                wait_bytes(gat.at[b, pl.ds(0, 2)], at)
+            if dz == 1:
+                pieces = pwv.at[b, pl.ds(0, SIDE - 1)]
+                wait_bytes(pieces, rsem.at[base + WEIGHT_SEM])
+            rows = jnp.concatenate([gat[b, 2 * zz], gat[b, 2 * zz + 1]], axis=0)
+            partial = partial + jnp.dot(
+                rows, pwv[b, zz], preferred_element_type=F32
+            )
+        osend[b] = partial
+
+        for dx in (2, 1, 3):
+            xx = (x + dx) % SIDE
+            rows = pl.ds(pl.multiple_of(xx * TROWS, TROWS), TROWS)
+            t = z * SIDE + xx
+            send(osend.at[b, rows], orecv.at[b, x], base + OUT_SEM, "tp", t)
         if b == 0:
             split_cells(1)
-
-        orecv[me_t] = osend[own_t]
-        wait_bytes(orecv.at[pl.ds(0, TP - 1)], rsem.at[base + OUT_SEM])
-        rows_sum = orecv[0].astype(F32)
-        for i in range(1, TP):
-            rows_sum = rows_sum + orecv[i].astype(F32)
+        rows = pl.ds(pl.multiple_of(x * TROWS, TROWS), TROWS)
+        orecv[b, x] = osend[b, rows]
+        wait_bytes(orecv.at[b, pl.ds(0, SIDE - 1)], rsem.at[base + OUT_SEM])
+        rows_sum = orecv[b, 0] + orecv[b, 1] + (orecv[b, 2] + orecv[b, 3])
         if b + 1 < NB:
             g[b + 1, own_t] = rows_sum.astype(BF16)
             gather_rows(b + 1)
@@ -379,9 +407,17 @@
         for i in range(5):
             pieces = yrecv.at[b, 0, pl.ds(0, 3 * TILES[i][1])]
             wait_bytes(pieces, ssem.at[base + CHIP_SEM + i])
-        pieces = gat.at[b, pl.ds(0, (DP - 1) * DROWS)]
-        wait_bytes(pieces, ssem.at[base + GATED_SEM + y])
-        wait_bytes(outs[b][1].at[pl.ds(0, TP - 1)], ssem.at[base + OUT_SEM])
+
+        @pl.when(y == z)
+        def _():
+            wait_bytes(gat.at[b, pl.ds(0, DP - 1)], ssem.at[base + GATED_SEM])
+
+        @pl.when(y != z)
+        def _():
+            wait_bytes(gat.at[b], ssem.at[base + GATED_SEM])
+
+        wait_bytes(orecv.at[b, pl.ds(0, SIDE - 1)], ssem.at[base + OUT_SEM])
+        wait_bytes(pwv.at[b, pl.ds(0, SIDE - 1)], ssem.at[base + WEIGHT_SEM])
     for store in stores:
         store.wait()
 
@@ -445,7 +481,7 @@
             pltpu.VMEM((NB, COLS, QKVO), BF16),
             pltpu.VMEM((2, NB, TP, COLS), BF16),
             pltpu.VMEM((NB, TP, COLS), BF16),
-            pltpu.VMEM((NB, DH, COLS), BF16),
+            pltpu.VMEM((NB, SIDE, DH, COLS), BF16),
             pltpu.VMEM((NB, COLS), F32),
             pltpu.VMEM((NB, DH), F32),
             pltpu.VMEM((NB, DROWS, DH), F32),
@@ -457,15 +493,14 @@
             pltpu.VMEM((NB, SIDE, TALL, DH), F32),
             pltpu.VMEM((DROWS // 8, 16, DH), BF16),
             pltpu.VMEM((2 * DROWS, DH), F32),
-            pltpu.VMEM((NB, ROWS, DH), BF16),
-            pltpu.VMEM((ROWS, COLS), F32),
-            pltpu.VMEM((ROWS, COLS), BF16),
-            pltpu.VMEM((TP, TROWS, COLS), F32),
-            pltpu.VMEM((TP, TROWS, COLS), BF16),
+            pltpu.VMEM((NB, DROWS, DH), BF16),
+            pltpu.VMEM((NB, DP, DROWS, DH), BF16),
+            pltpu.VMEM((NB, GROUP, COLS), F32),
+            pltpu.VMEM((NB, SIDE, TROWS, COLS), F32),
             pltpu.VMEM((TROWS, COLS), BF16),
             pltpu.VMEM((NB, DROWS, DH), F32),
             pltpu.VMEM((NB, DROWS), F32),
-            pltpu.SemaphoreType.DMA((14,)),
+            pltpu.SemaphoreType.DMA((15,)),
             pltpu.SemaphoreType.DMA((NB + 3,)),
             pltpu.SemaphoreType.DMA((SEMS * NB,)),
             pltpu.SemaphoreType.DMA((SEMS * NB,)),

time: 59.2 us -> 55.5 us (0.938)
  Pallas kernels: 58.4 us -> 54.3 us
    pallas_call x1, Pallas kernels: 54.5 us -> 50.3 us  [per_device(): pl.pallas_call(mega, out_shape=results, in_specs=[anywhere] * 13, out_spe...]
where the time goes in v4:
time: 55.5 us; the launch traced here: 54.9 us
  Pallas kernels  54.3 us (98%)
  between operations  0.64 us (1%)
    pallas_call x1, Pallas kernels, per_device(): pl.pallas_call(mega, out_shape=results, in_specs=[anywhere] * 13, out_spe...  50.3 us
    pallas_call x1, Pallas kernels, per_device(): pl.pallas_call(hand_on, out_shape=results, in_specs=[anywhere] * 4, out_s...  3.91 us

profile of v4, /device:TPU:1, one launch (start us, length us, event | category | flops | bytes accessed | tf_op | source)
XLA Modules:
  0.0 54.9 jit_solution(5461048699575924473)
XLA Ops:
  0.6 50.3 %two_blocks.1 = (bf16[16,512]{1,0:T(8,128)(2,1)}, f32[2,32,128,128]{3,2,1,0:T(8,128)}, f32[2,32,128]{2,1,0:T(8,128)}, f32[2,32]{1,0:T(2,128)}) custom-call(bf16[16,512]{1,0:T(8,128)(2,1)} %tok.1, bf16[2,512,128]{2,1,0:T(8,128)(2,1)} %qw.1, bf16[2,512,128]{2,1,0:T(8,128)(2,1)} %kw.1, bf16[2,512,128]{2,1,0:T(8,128)(2,1)} %vw.1, bf16[2,512,128]{2,1,0:T(8,128)(2,1)} %ow.1, ...), custom_call_target="tpu_custom_call" | custom-call | tf_op jit(solution)/shard_map/two_blocks/pallas_call | solution.py:474
  51.0 3.9 %hand_on.1 = (bf16[16,512]{1,0:T(8,128)(2,1)}, f32[2,32,128,128]{3,2,1,0:T(8,128)}, f32[2,32,128]{2,1,0:T(8,128)}, f32[2,32]{1,0:T(2,128)}) custom-call(bf16[16,512]{1,0:T(8,128)(2,1)} %get-tuple-element.12.final, f32[2,32,128,128]{3,2,1,0:T(8,128)} %get-tuple-element.13.cell, f32[2,32,128]{2,1,0:T(8,128)} %get-tuple-element.14.normer, ...), custom_call_target="tpu_custom_call" | custom-call | tf_op jit(solution)/shard_map/hand_on/pallas_call | solution.py:528
